TPU v7x, 32 devices: a whole 2x2x4 slice. The times are simulated.
32 devices in a mesh: sp: 8 (over z, y), tp: 4 (over x, core).
Axes of the slice: x: 2, y: 2, z: 4, core: 2. Of those that a mesh axis runs over, the one named last changes fastest.
Arguments:
- queries: bfloat16 [4096, 2048], P('sp', 'tp'), may hold values from -8 to 8
- keys: bfloat16 [4096, 512], P('sp', 'tp'), may hold values from -8 to 8
- values: bfloat16 [4096, 512], P('sp', 'tp'), may hold values from -6 to 6
- q_gain: float32 [128], replicated, may hold values from 0.1 to 5.8
- k_gain: float32 [128], replicated, may hold values from 0.1 to 5.8
- out_weight: bfloat16 [2048, 2048], replicated, may hold values from -0.125 to 0.125
- out_gain: float32 [2048], replicated, may hold values from 0.1 to 1.9
- residual_in: bfloat16 [4096, 2048], P(('sp', 'tp')), may hold values from -6 to 6
- mlp_gain: float32 [2048], replicated, may hold values from 0.1 to 1.9
- gate_weight: bfloat16 [2048, 5632], P('sp', 'tp'), may hold values from -0.125 to 0.125
- up_weight: bfloat16 [2048, 5632], P('sp', 'tp'), may hold values from -0.125 to 0.125
- down_weight: bfloat16 [5632, 2048], P('tp', 'sp'), may hold values from -0.078125 to 0.078125
- final_gain: float32 [2048], replicated, may hold values from 0.1 to 1.9
Outputs:
- layer_out: bfloat16 [4096, 2048], P(('sp', 'tp'))
All inputs are finite; a program needn't handle non-finite values.
Results may differ from a plain program's by a relative error of at most 0.015.
The roundings to bfloat16 on the way count: a program that leaves them out, or rounds other values in their place, can miss the bound.
Values may be sent and summed in bfloat16 or wider, within the bound.
A program may use at most 128 MiB of HBM per device.

v0:
```python
import functools
import math

import jax
import jax.numpy as jnp
from jax import lax
from jax.experimental import pallas as pl
from jax.experimental.pallas import tpu as pltpu
from jax.sharding import PartitionSpec as P

GRID_W = 64


def rms_scale(matrix):
    return matrix * lax.rsqrt(jnp.mean(matrix * matrix, axis=-1, keepdims=True) + 1e-06)


def rotary(matrix, positions):
    quarter = matrix.shape[-1] // 4
    freqs = 10000.0 ** (-jnp.arange(quarter, dtype=jnp.float32) / quarter)
    grid = jnp.stack([positions // GRID_W, positions % GRID_W], axis=-1).astype(jnp.float32)
    angle = grid[:, :, None] * freqs
    cosine = jnp.cos(angle)[:, None]
    sine = jnp.sin(angle)[:, None]
    parts = matrix.reshape(matrix.shape[:-1] + (2, 2, quarter))
    first = parts[..., 0, :]
    second = parts[..., 1, :]
    turned = jnp.stack([first * cosine - second * sine, second * cosine + first * sine], axis=-2)
    return turned.reshape(matrix.shape)


def on_device(
    queries,
    keys,
    values,
    q_gain,
    k_gain,
    out_weight,
    out_gain,
    residual_in,
    mlp_gain,
    gate_weight,
    up_weight,
    down_weight,
    final_gain,
):
    tok_rows = queries.shape[0]
    head_size = q_gain.shape[0]
    q_heads = queries.shape[1] // head_size
    kv_heads = keys.shape[1] // head_size
    group_size = q_heads // kv_heads
    positions = lax.axis_index("sp") * tok_rows + jnp.arange(tok_rows, dtype=jnp.int32)
    query_rot = rotary(
        rms_scale(queries.reshape(tok_rows, q_heads, head_size).astype(jnp.float32)) * q_gain,
        positions,
    ).astype(jnp.bfloat16)
    key_rot = rotary(
        rms_scale(keys.reshape(tok_rows, kv_heads, head_size).astype(jnp.float32)) * k_gain,
        positions,
    ).astype(jnp.bfloat16)
    key_flat = key_rot.reshape(tok_rows, kv_heads * head_size)
    grouped = query_rot.reshape(tok_rows, kv_heads, group_size, head_size)
    score_scale = head_size ** (-0.5)
    key_all, value_all = (
        lax.all_gather(key_flat, "sp", axis=0, tiled=True),
        lax.all_gather(values, "sp", axis=0, tiled=True),
    )
    total_rows = key_all.shape[0]
    span = math.gcd(total_rows, 1024)
    key_blocks = key_all.reshape(total_rows // span, span, kv_heads, head_size)
    value_blocks = value_all.reshape(total_rows // span, span, kv_heads, head_size)

    def step(run_state, blocks):
        highest, weight_sum, accum = run_state
        key_block, value_block = blocks
        scores = (
            jnp.einsum("qcgd,kcd->cgqk", grouped, key_block, preferred_element_type=jnp.float32)
            * score_scale
        )
        new_high = jnp.maximum(highest, jnp.max(scores, axis=-1))
        factor = jnp.exp(highest - new_high)
        exp_scores = jnp.exp(scores - new_high[..., None])
        weight_sum = weight_sum * factor + jnp.sum(exp_scores, axis=-1)
        accum = accum * factor[..., None] + jnp.einsum(
            "cgqk,kcd->cgqd",
            exp_scores.astype(jnp.bfloat16),
            value_block,
            preferred_element_type=jnp.float32,
        )
        return ((new_high, weight_sum, accum), None)

    start_state = (
        jnp.full((kv_heads, group_size, tok_rows), -1e30, jnp.float32),
        jnp.zeros((kv_heads, group_size, tok_rows), jnp.float32),
        jnp.zeros((kv_heads, group_size, tok_rows, head_size), jnp.float32),
    )
    final_state, unused = lax.scan(step, start_state, (key_blocks, value_blocks))
    highest, weight_sum, accum = final_state
    attended = (
        jnp.transpose(accum / weight_sum[..., None], (2, 0, 1, 3))
        .reshape(tok_rows, q_heads * head_size)
        .astype(jnp.bfloat16)
    )
    head_rows = lax.all_to_all(attended, "tp", split_axis=0, concat_axis=1, tiled=True)
    projected = jnp.dot(head_rows, out_weight, preferred_element_type=jnp.float32)
    mid_stream = (residual_in.astype(jnp.float32) + out_gain * rms_scale(projected)).astype(
        jnp.bfloat16
    )
    normed = (mlp_gain * rms_scale(mid_stream.astype(jnp.float32))).astype(jnp.bfloat16)
    mixer_in = lax.all_gather(normed, "tp", axis=0, tiled=True)
    gate_proj = jnp.dot(
        mixer_in,
        lax.all_gather(gate_weight, "sp", axis=0, tiled=True),
        preferred_element_type=jnp.float32,
    )
    up_proj = jnp.dot(
        mixer_in,
        lax.all_gather(up_weight, "sp", axis=0, tiled=True),
        preferred_element_type=jnp.float32,
    )
    down_full = lax.all_gather(down_weight, "sp", axis=1, tiled=True)
    hidden = (jax.nn.silu(gate_proj) * up_proj).astype(jnp.bfloat16)
    mlp_branch = lax.psum_scatter(
        jnp.dot(hidden, down_full, preferred_element_type=jnp.float32).astype(jnp.bfloat16),
        "tp",
        scatter_dimension=0,
        tiled=True,
    ).astype(jnp.float32)
    return (mid_stream.astype(jnp.float32) + final_gain * rms_scale(mlp_branch)).astype(
        jnp.bfloat16
    )


MESH = pl.DeviceIdType.MESH
EPS = 1e-06


def layer_kernel(
    n,
    tn,
    q_in,
    k_in,
    v_hbm,
    cos_ref,
    sin_ref,
    qg_ref,
    kg_ref,
    ow_hbm,
    og_ref,
    res_ref,
    mg_ref,
    gate_hbm,
    up_hbm,
    down_hbm,
    fg_ref,
    out_ref,
    qs,
    kbuf,
    vbuf,
    raw,
    wt,
    wall,
    ow,
    m_s,
    l_s,
    acc,
    att,
    heads,
    proj,
    mid,
    toks,
    osc,
    psend,
    precv,
    loc_sem,
    send_sem,
    recv_sem,
    tp_send,
    tp_recv,
    a_send,
    a_recv,
    w_send,
    w_recv,
    t_send,
    t_recv,
    p_send,
    p_recv,
):
    sp = lax.axis_index("sp")
    tp = lax.axis_index("tp")
    half = n // 2

    def ring_at(pos):
        pos = lax.rem(pos + 2 * n, n)
        return jnp.where(pos < half, 2 * pos, 2 * (n - 1 - pos) + 1)

    pos = jnp.where(lax.rem(sp, 2) == 0, sp // 2, n - 1 - sp // 2)
    right, left = ring_at(pos + 1), ring_at(pos - 1)
    tok, hd = k_in.shape
    groups = q_in.shape[1] // hd
    depth = gate_hbm.shape[0]
    hidden = gate_hbm.shape[1]
    rows = res_ref.shape[0]
    width = groups * hd
    chunk = hidden // n
    side = rows // 2

    locs = {
        "v": pltpu.make_async_copy(v_hbm, vbuf.at[sp], loc_sem.at[0]),
        "g": pltpu.make_async_copy(gate_hbm, raw.at[0], loc_sem.at[1]),
        "u": pltpu.make_async_copy(up_hbm, raw.at[1], loc_sem.at[2]),
        "d": pltpu.make_async_copy(down_hbm, wt.at[2], loc_sem.at[3]),
        "o": pltpu.make_async_copy(ow_hbm, ow, loc_sem.at[4]),
    }
    for name in "vgudo":
        locs[name].start()

    lane = lax.broadcasted_iota(jnp.int32, (tok, hd), 1)
    quarter = hd // 4
    first = lax.rem(lane, 2 * quarter) < quarter

    def turned(x, gain):
        x = x.astype(jnp.float32)
        x = x * lax.rsqrt(jnp.mean(x * x, axis=-1, keepdims=True) + EPS) * gain
        other = jnp.where(first, pltpu.roll(x, hd - quarter, 1), pltpu.roll(x, quarter, 1))
        return (x * cos_ref[...] + other * sin_ref[...]).astype(jnp.bfloat16)

    kbuf[sp] = turned(k_in[...], kg_ref[...])

    barrier = pltpu.get_barrier_semaphore()
    for d in range(1, n):
        pl.semaphore_signal(
            barrier, inc=1, device_id=(lax.rem(sp + d, n), tp), device_id_type=MESH
        )
    for d in range(1, tn):
        pl.semaphore_signal(
            barrier, inc=1, device_id=(sp, lax.rem(tp + d, tn)), device_id_type=MESH
        )
    pl.semaphore_wait(barrier, n - 1 + tn - 1)

    items = {
        "k": (0, half, lambda s: kbuf.at[s]),
        "v": (1, half - 1, lambda s: vbuf.at[s]),
    }
    started = []

    def copies(name, step):
        number, to_right, view = items[name]
        found = []
        for way, count in ((0, to_right), (1, n - 1 - to_right)):
            if step > count:
                continue
            origin = ring_at(pos - (step - 1)) if way == 0 else ring_at(pos + (step - 1))
            index = (number * 2 + way) * half + step - 1
            found.append(
                pltpu.make_async_remote_copy(
                    src_ref=view(origin),
                    dst_ref=view(origin),
                    send_sem=send_sem.at[index],
                    recv_sem=recv_sem.at[index],
                    device_id=(right if way == 0 else left, tp),
                    device_id_type=MESH,
                )
            )
        return found

    def send(name, step):
        for copy in copies(name, step):
            copy.start()
            started.append(copy)

    def arrive(name, step, then=True):
        number, to_right, view = items[name]
        for way, count in ((0, to_right), (1, n - 1 - to_right)):
            if step > count:
                continue
            origin = ring_at(pos - step) if way == 0 else ring_at(pos + step)
            index = (number * 2 + way) * half + step - 1
            pltpu.make_async_remote_copy(
                src_ref=view(origin),
                dst_ref=view(origin),
                send_sem=send_sem.at[index],
                recv_sem=recv_sem.at[index],
                device_id=(right if way == 0 else left, tp),
                device_id_type=MESH,
            ).wait_recv()
            if step < count:
                index += 1
                copy = pltpu.make_async_remote_copy(
                    src_ref=view(origin),
                    dst_ref=view(origin),
                    send_sem=send_sem.at[index],
                    recv_sem=recv_sem.at[index],
                    device_id=(right if way == 0 else left, tp),
                    device_id_type=MESH,
                )
                copy.start()
                started.append(copy)

    send("k", 1)
    locs["v"].wait()
    send("v", 1)
    locs["g"].wait()
    locs["u"].wait()

    def transpose(i, carry):
        part = pl.ds(pl.multiple_of(i * 128, 128), 128)
        for which in range(2):
            wt[which, part, :] = raw[which, :, part].T
        return carry

    lax.fori_loop(0, hidden // 128, transpose, 0)
    locs["d"].wait()

    def units(index):
        return pl.ds(pl.multiple_of(index * chunk, 16), chunk)

    own_piece = pltpu.make_async_copy(
        wt.at[:, units(sp), :], wall.at[sp, :, units(tp), :], loc_sem.at[5]
    )
    own_piece.start()

    def spread(d):
        peer = lax.rem(sp + d, n)
        copy = pltpu.make_async_remote_copy(
            src_ref=wt.at[:, units(peer), :],
            dst_ref=wall.at[sp, :, units(tp), :],
            send_sem=a_send.at[d - 1],
            recv_sem=a_recv.at[d - 1],
            device_id=(peer, tp),
            device_id_type=MESH,
        )
        copy.start()
        started.append(copy)

    across, beside = lax.rem(tp + tn // 2, tn), tp + 1 - 2 * lax.rem(tp, 2)

    def relay(kind, d):
        slot = lax.rem(sp - d + n, n)
        owner = across if kind == 2 else tp
        piece = wall.at[slot, :, units(owner), :]
        return pltpu.make_async_remote_copy(
            src_ref=piece,
            dst_ref=piece,
            send_sem=w_send.at[kind * n + d],
            recv_sem=w_recv.at[kind * n + d],
            device_id=(sp, across if kind == 0 else beside),
            device_id_type=MESH,
        )

    def pass_on(d):
        if d == 0:
            own_piece.wait()
        else:
            slot = lax.rem(sp - d + n, n)
            piece = wall.at[slot, :, units(tp), :]
            pltpu.make_async_remote_copy(
                src_ref=piece,
                dst_ref=piece,
                send_sem=a_send.at[d - 1],
                recv_sem=a_recv.at[d - 1],
                device_id=(lax.rem(sp + d, n), tp),
                device_id_type=MESH,
            ).wait_recv()
        for kind in (0, 1):
            copy = relay(kind, d)
            copy.start()
            started.append(copy)

    spread(1)
    spread(2)
    pass_on(0)

    for h in range(groups):
        qs[h] = turned(q_in[:, h * hd : (h + 1) * hd], qg_ref[...])
    m_s[...] = jnp.full_like(m_s, -1e30)
    l_s[...] = jnp.zeros_like(l_s)
    acc[...] = jnp.zeros_like(acc)
    factor = hd ** (-0.5) * math.log2(math.e)

    def attend(slots):
        def one(i, carry):
            h = lax.rem(i, groups)
            slot = slots[0]
            if len(slots) > 1:
                slot = jnp.where(i < groups, slots[0], slots[1])
            scores = lax.dot_general(
                qs[h], kbuf[slot], (((1,), (1,)), ((), ())), preferred_element_type=jnp.float32
            )
            before = m_s[h]
            highest = jnp.maximum(before, jnp.max(scores, axis=-1, keepdims=True))
            scale = jnp.exp2((before - highest) * factor)
            probs = jnp.exp2((scores - highest) * factor)
            m_s[h] = highest
            l_s[h] = l_s[h] * scale + jnp.sum(probs, axis=-1, keepdims=True)
            acc[h] = acc[h] * scale + jnp.dot(
                probs.astype(jnp.bfloat16), vbuf[slot], preferred_element_type=jnp.float32
            )
            return carry

        lax.fori_loop(0, groups * len(slots), one, 0)

    attend([sp])
    for step in range(1, half + 1):
        arrive("k", step)
        arrive("v", step)
        for d in (2 * step + 1, 2 * step + 2):
            if d < n:
                spread(d)
        ends = [ring_at(pos - step), ring_at(pos + step)]
        attend(ends if step < half else ends[:1])
        for d in (2 * step - 5, 2 * step - 4):
            if 0 < d < n:
                pass_on(d)

    for h in range(groups):
        done = (acc[h] / l_s[h]).astype(jnp.bfloat16)
        for t in range(tn):
            att[t, :, h * hd : (h + 1) * hd] = done[t * rows : (t + 1) * rows]
    to_heads = []
    for d in range(1, tn):
        peer = lax.rem(tp + d, tn)
        copy = pltpu.make_async_remote_copy(
            src_ref=att.at[peer],
            dst_ref=heads.at[tp],
            send_sem=tp_send.at[d - 1],
            recv_sem=tp_recv.at[d - 1],
            device_id=(sp, peer),
            device_id_type=MESH,
        )
        copy.start()
        to_heads.append(copy)
    heads[tp] = att[tp]
    for d in range(2 * half - 3, n):
        pass_on(d)
    locs["o"].wait()
    for copy in to_heads:
        copy.wait_recv()

    span = math.gcd(ow.shape[1], 512)

    def project(i, carry):
        cols = pl.ds(pl.multiple_of(i * span, span), span)
        total = jnp.zeros((rows, span), jnp.float32)
        for t in range(tn):
            total += jnp.dot(
                heads[t], ow[t * width : (t + 1) * width, cols], preferred_element_type=jnp.float32
            )
        proj[:, cols] = total
        return carry

    lax.fori_loop(0, ow.shape[1] // span, project, 0)
    projected = proj[...]
    middle = (
        res_ref[...].astype(jnp.float32)
        + og_ref[...]
        * (projected * lax.rsqrt(jnp.mean(projected * projected, axis=-1, keepdims=True) + EPS))
    ).astype(jnp.bfloat16)
    mid[...] = middle
    middle = middle.astype(jnp.float32)
    normed = (
        mg_ref[...] * (middle * lax.rsqrt(jnp.mean(middle * middle, axis=-1, keepdims=True) + EPS))
    ).astype(jnp.bfloat16)

    for way in range(2):
        toks[way, sp] = normed[way * side : (way + 1) * side]

    def token_copy(way, step):
        origin = ring_at(pos - (step - 1)) if way == 0 else ring_at(pos + (step - 1))
        return pltpu.make_async_remote_copy(
            src_ref=toks.at[way, origin],
            dst_ref=toks.at[way, origin],
            send_sem=t_send.at[way * n + step],
            recv_sem=t_recv.at[way * n + step],
            device_id=(right if way == 0 else left, tp),
            device_id_type=MESH,
        )

    def sum_copy(way, step):
        return pltpu.make_async_remote_copy(
            src_ref=psend.at[way, step],
            dst_ref=precv.at[way, step],
            send_sem=p_send.at[way * n + step],
            recv_sem=p_recv.at[way * n + step],
            device_id=(right if way == 0 else left, tp),
            device_id_type=MESH,
        )

    for way in range(2):
        token_copy(way, 1).start()
    for d in range(n):
        relay(0, d).wait_recv()
        copy = relay(2, d)
        copy.start()
        started.append(copy)
    for d in range(n):
        relay(1, d).wait_recv()
        relay(2, d).wait_recv()

    def block(step, carry):
        for way in range(2):

            @pl.when(step > 0)
            def _():
                token_copy(way, step).wait_recv()

            @pl.when(jnp.logical_and(step > 0, step < n - 1))
            def _():
                token_copy(way, step + 1).start()

        tokens = jnp.concatenate(
            [toks[0, ring_at(pos - step)], toks[1, ring_at(pos + step)]], axis=0
        )
        branches = []
        for which in range(2):
            total = jnp.zeros((rows, hidden // n * tn), jnp.float32)
            for s in range(n):
                total += lax.dot_general(
                    tokens[:, s * depth : (s + 1) * depth],
                    wall[s, which],
                    (((1,), (1,)), ((), ())),
                    preferred_element_type=jnp.float32,
                )
            branches.append(total)
        gate, up = branches
        inner = (gate / (1.0 + jnp.exp(-gate)) * up).astype(jnp.bfloat16)
        for s in range(n):
            osc[:, s * depth : (s + 1) * depth] = jnp.dot(
                inner, wall[s, 2], preferred_element_type=jnp.float32
            )

        @pl.when(step == 0)
        def _():
            proj[...] = osc[...]

        @pl.when(step > 0)
        def _():
            for way in range(2):
                part = slice(way * side, (way + 1) * side)

                @pl.when(step > 1)
                def _():
                    sum_copy(way, step - 1).wait_recv()
                    osc[part] += precv[way, step - 1].astype(jnp.float32)

                psend[way, step] = osc[part].astype(jnp.bfloat16)
                sum_copy(way, step).start()

        return carry

    lax.fori_loop(0, n, block, 0)
    for way in range(2):
        sum_copy(way, n - 1).wait_recv()
        part = slice(way * side, (way + 1) * side)
        proj[part] += precv[way, n - 1].astype(jnp.float32)
    total = proj[...]
    out_ref[...] = (
        mid[...].astype(jnp.float32)
        + fg_ref[...] * (total * lax.rsqrt(jnp.mean(total * total, axis=-1, keepdims=True) + EPS))
    ).astype(jnp.bfloat16)
    for copy in started + to_heads:
        copy.wait_send()

    def drain(step, carry):
        for way in range(2):
            token_copy(way, step).wait_send()
            sum_copy(way, step).wait_send()
        return carry

    lax.fori_loop(1, n, drain, 0)


def rotary_tables(tok_rows, head_size):
    quarter = head_size // 4
    positions = lax.axis_index("sp") * tok_rows + jnp.arange(tok_rows, dtype=jnp.int32)
    lane = jnp.arange(head_size, dtype=jnp.int32)
    freqs = 10000.0 ** (-(lane % quarter).astype(jnp.float32) / quarter)
    row = (positions // GRID_W).astype(jnp.float32)[:, None]
    column = (positions % GRID_W).astype(jnp.float32)[:, None]
    angle = jnp.where(lane < 2 * quarter, row, column) * freqs
    sine = jnp.sin(angle)
    return jnp.cos(angle), jnp.where(lane % (2 * quarter) < quarter, -sine, sine)


def fused(n, tn, *args):
    (queries, keys, values, q_gain, k_gain, out_weight, out_gain, residual_in) = args[:8]
    (mlp_gain, gate_weight, up_weight, down_weight, final_gain) = args[8:]
    tok, hd = keys.shape
    groups = queries.shape[1] // hd
    depth, hidden = gate_weight.shape
    rows, wide = residual_in.shape
    cosine, sine = rotary_tables(tok, hd)
    vmem = pl.BlockSpec(memory_space=pltpu.VMEM)
    hbm = pl.BlockSpec(memory_space=pl.ANY)
    half = n // 2
    b16, f32 = jnp.bfloat16, jnp.float32
    return pl.pallas_call(
        functools.partial(layer_kernel, n, tn),
        out_shape=jax.ShapeDtypeStruct((rows, wide), b16),
        in_specs=[vmem, vmem, hbm, vmem, vmem, vmem, vmem, hbm, vmem, vmem, vmem, hbm, hbm, hbm, vmem],
        out_specs=vmem,
        scratch_shapes=[
            pltpu.VMEM((groups, tok, hd), b16),
            pltpu.VMEM((n, tok, hd), b16),
            pltpu.VMEM((n, tok, hd), b16),
            pltpu.VMEM((2, depth, hidden), b16),
            pltpu.VMEM((3, hidden, depth), b16),
            pltpu.VMEM((n, 3, hidden // n * tn, depth), b16),
            pltpu.VMEM((wide, wide), b16),
            pltpu.VMEM((groups, tok, 1), f32),
            pltpu.VMEM((groups, tok, 1), f32),
            pltpu.VMEM((groups, tok, hd), f32),
            pltpu.VMEM((tn, rows, groups * hd), b16),
            pltpu.VMEM((tn, rows, groups * hd), b16),
            pltpu.VMEM((rows, wide), f32),
            pltpu.VMEM((rows, wide), b16),
            pltpu.VMEM((2, n, rows // 2, wide), b16),
            pltpu.VMEM((rows, wide), f32),
            pltpu.VMEM((2, n, rows // 2, wide), b16),
            pltpu.VMEM((2, n, rows // 2, wide), b16),
            pltpu.SemaphoreType.DMA((6,)),
            pltpu.SemaphoreType.DMA((4 * half,)),
            pltpu.SemaphoreType.DMA((4 * half,)),
            pltpu.SemaphoreType.DMA((tn - 1,)),
            pltpu.SemaphoreType.DMA((tn - 1,)),
            pltpu.SemaphoreType.DMA((n - 1,)),
            pltpu.SemaphoreType.DMA((n - 1,)),
            pltpu.SemaphoreType.DMA((3 * n,)),
            pltpu.SemaphoreType.DMA((3 * n,)),
            pltpu.SemaphoreType.DMA((2 * n,)),
            pltpu.SemaphoreType.DMA((2 * n,)),
            pltpu.SemaphoreType.DMA((2 * n,)),
            pltpu.SemaphoreType.DMA((2 * n,)),
        ],
        compiler_params=pltpu.CompilerParams(
            collective_id=0, has_side_effects=True, vmem_limit_bytes=67043328
        ),
    )(
        queries,
        keys,
        values,
        cosine,
        sine,
        q_gain[None],
        k_gain[None],
        out_weight,
        out_gain[None],
        residual_in,
        mlp_gain[None],
        gate_weight,
        up_weight,
        down_weight,
        final_gain[None],
    )


def body(mesh, *args):
    n, tn = mesh.shape["sp"], mesh.shape["tp"]
    tok, hd = args[1].shape
    depth, hidden = args[9].shape
    fits = n % 2 == 0 and 4 <= n <= 8 and depth % 128 == 0 and hidden % 128 == 0
    fits = fits and tn == 4 and hidden % (16 * n) == 0 and args[7].shape[0] % 32 == 0
    if fits and tok % 256 == 0 and hd == 128:
        return fused(n, tn, *args)
    return on_device(*args)


def solution(mesh):
    return jax.shard_map(
        functools.partial(body, mesh),
        mesh=mesh,
        in_specs=(
            P("sp", "tp"),
            P("sp", "tp"),
            P("sp", "tp"),
            P(),
            P(),
            P(),
            P(),
            P(("sp", "tp"), None),
            P(),
            P("sp", "tp"),
            P("sp", "tp"),
            P("tp", "sp"),
            P(),
        ),
        out_specs=P(("sp", "tp"), None),
        check_vma=False,
    )
```

profile of v0, /device:TPU:0, one launch (start us, length us, event | category | flops | bytes accessed | tf_op | source)
XLA Modules:
  0.0 211.9 jit_solution(15836255444106876130)
XLA Ops:
  0.0 1.9 negate_select_fusion
  1.9 208.2 %shard_map.127 = bf16[128,2048]{1,0:T(8,128)(2,1)} custom-call(bf16[512,512]{1,0:T(8,128)(2,1)} %q_in.1, bf16[512,128]{1,0:T(8,128)(2,1)} %k_in.1, bf16[512,128]{1,0:T(8,128)(2,1)} %v_hbm.1, f32[512,128]{1,0:T(8,128)} %get-tuple-element.6.cos_ref, f32[512,128]{1,0:T(8,128)} %get-tuple-element.5.sin_ref, f32[1,128]{1,0:T(1,128)} %bitcast.8, ...), custom_call_target="tpu_custom_call" | custom-call | tf_op jit(solution)/shard_map/pallas_call | solution.py:597
  210.0 1.9 copy.15
  (3 shorter events, 0.0 us)
where the time goes:
time: 215 us; the launch traced here: 212 us
  Pallas kernels  208 us (97%)
    pallas_call x1, Pallas kernels, fused(): pl.pallas_call(functools.partial(layer_kernel, n, tn), out_shape=jax.Shap...  208 us

commit v1 on v0

--- a/solution.py
+++ b/solution.py
@@ -157,6 +157,7 @@
     qs,
     kbuf,
     vbuf,
+    vraw,
     raw,
     wt,
     wall,
@@ -169,6 +170,7 @@
     proj,
     mid,
     toks,
+    inner,
     osc,
     psend,
     precv,
@@ -177,8 +179,6 @@
     recv_sem,
     tp_send,
     tp_recv,
-    a_send,
-    a_recv,
     w_send,
     w_recv,
     t_send,
@@ -189,24 +189,30 @@
     sp = lax.axis_index("sp")
     tp = lax.axis_index("tp")
     half = n // 2
+    nz = n // 2
 
     def ring_at(pos):
         pos = lax.rem(pos + 2 * n, n)
         return jnp.where(pos < half, 2 * pos, 2 * (n - 1 - pos) + 1)
 
-    pos = jnp.where(lax.rem(sp, 2) == 0, sp // 2, n - 1 - sp // 2)
+    z, y = sp // 2, lax.rem(sp, 2)
+    pos = jnp.where(y == 0, z, n - 1 - z)
     right, left = ring_at(pos + 1), ring_at(pos - 1)
+    other_y = 1 - y
+    y_dev = (sp + 1 - 2 * y, tp)
+    x_dev = (sp, lax.rem(tp + tn // 2, tn))
+    c_dev = (sp, tp + 1 - 2 * lax.rem(tp, 2))
     tok, hd = k_in.shape
     groups = q_in.shape[1] // hd
     depth = gate_hbm.shape[0]
     hidden = gate_hbm.shape[1]
-    rows = res_ref.shape[0]
+    rows, wide = res_ref.shape
     width = groups * hd
-    chunk = hidden // n
-    side = rows // 2
+    hq = hidden // nz
+    units = hq * tn
 
     locs = {
-        "v": pltpu.make_async_copy(v_hbm, vbuf.at[sp], loc_sem.at[0]),
+        "v": pltpu.make_async_copy(v_hbm, vraw, loc_sem.at[0]),
         "g": pltpu.make_async_copy(gate_hbm, raw.at[0], loc_sem.at[1]),
         "u": pltpu.make_async_copy(up_hbm, raw.at[1], loc_sem.at[2]),
         "d": pltpu.make_async_copy(down_hbm, wt.at[2], loc_sem.at[3]),
@@ -238,68 +244,141 @@
         )
     pl.semaphore_wait(barrier, n - 1 + tn - 1)
 
+    started = []
+
+    def start(copy):
+        copy.start()
+        started.append(copy)
+
     items = {
         "k": (0, half, lambda s: kbuf.at[s]),
         "v": (1, half - 1, lambda s: vbuf.at[s]),
     }
-    started = []
-
-    def copies(name, step):
+
+    def ring_copy(name, way, step, origin):
         number, to_right, view = items[name]
-        found = []
-        for way, count in ((0, to_right), (1, n - 1 - to_right)):
+        index = (number * 2 + way) * half + step - 1
+        return pltpu.make_async_remote_copy(
+            src_ref=view(origin),
+            dst_ref=view(origin),
+            send_sem=send_sem.at[index],
+            recv_sem=recv_sem.at[index],
+            device_id=(right if way == 0 else left, tp),
+            device_id_type=MESH,
+        )
+
+    def counts(name):
+        to_right = items[name][1]
+        return ((0, to_right), (1, n - 1 - to_right))
+
+    def send(name):
+        for way, count in counts(name):
+            start(ring_copy(name, way, 1, sp))
+
+    def arrive(name, step):
+        for way, count in counts(name):
             if step > count:
                 continue
-            origin = ring_at(pos - (step - 1)) if way == 0 else ring_at(pos + (step - 1))
-            index = (number * 2 + way) * half + step - 1
-            found.append(
+            origin = ring_at(pos - step) if way == 0 else ring_at(pos + step)
+            ring_copy(name, way, step, origin).wait_recv()
+            if step < count:
+                start(ring_copy(name, way, step + 1, origin))
+
+    bases = {"z": 0, "x": 1, "y": 2, "d": 3, "cz": 4, "cy": 5, "cx": 6, "cd": 7}
+    grain = {k: [(0, 3)] for k in range(nz)}
+    grain[nz - 1] = [(0, 1), (1, 1), (2, 1)]
+
+    def column(k, side):
+        return 2 * lax.rem(z + k, nz) + side
+
+    def piece(slot, r, part):
+        return wall.at[slot, part[0] : part[0] + part[1], r * hq : (r + 1) * hq, :]
+
+    def weight_copy(kind, k, part):
+        index = (bases[kind] * nz + k) * 3 + part[0]
+        if kind == "x":
+            slot, r_from, r_to, dev = column(k, y), 0, 2, x_dev
+        elif kind == "y":
+            slot, r_from, r_to, dev = column(k, y), 0, 0, y_dev
+        elif kind == "d" and k % 2 == 0:
+            slot, r_from, r_to, dev = column(k, other_y), 0, 2, x_dev
+        elif kind == "d":
+            slot, r_from, r_to, dev = column(k, y), 2, 2, y_dev
+        else:
+            r_from = 0 if kind in ("cz", "cy") else 2
+            r_to, dev = r_from + 1, c_dev
+            slot = column(k, y if kind in ("cz", "cx") else other_y)
+        return pltpu.make_async_remote_copy(
+            src_ref=piece(slot, r_from, part),
+            dst_ref=piece(slot, r_to, part),
+            send_sem=w_send.at[index],
+            recv_sem=w_recv.at[index],
+            device_id=dev,
+            device_id_type=MESH,
+        )
+
+    def weight_wait(kind, k, part):
+        index = (bases[kind] * nz + k) * 3 + part[0]
+        side = y if kind in ("z", "x", "cz", "cx") else other_y
+        r = {"z": 0, "y": 0, "x": 2, "d": 2, "cz": 1, "cy": 1, "cx": 3, "cd": 3}[kind]
+        here = piece(column(k, side), r, part)
+        pltpu.make_async_remote_copy(
+            src_ref=here,
+            dst_ref=here,
+            send_sem=w_send.at[index],
+            recv_sem=w_recv.at[index],
+            device_id=c_dev,
+            device_id_type=MESH,
+        ).wait_recv()
+
+    spread_list = [(k, which) for k in range(1, nz) for which in range(3)]
+
+    def spread(count):
+        for k, which in spread_list[:count]:
+            target = lax.rem(z - k + nz, nz)
+            index = (bases["z"] * nz + k) * 3 + which
+            start(
                 pltpu.make_async_remote_copy(
-                    src_ref=view(origin),
-                    dst_ref=view(origin),
-                    send_sem=send_sem.at[index],
-                    recv_sem=recv_sem.at[index],
-                    device_id=(right if way == 0 else left, tp),
+                    src_ref=wt.at[
+                        which : which + 1, pl.ds(pl.multiple_of(target * hq, 16), hq), :
+                    ],
+                    dst_ref=wall.at[sp, which : which + 1, 0:hq, :],
+                    send_sem=w_send.at[index],
+                    recv_sem=w_recv.at[index],
+                    device_id=(2 * target + y, tp),
                     device_id_type=MESH,
                 )
             )
-        return found
-
-    def send(name, step):
-        for copy in copies(name, step):
-            copy.start()
-            started.append(copy)
-
-    def arrive(name, step, then=True):
-        number, to_right, view = items[name]
-        for way, count in ((0, to_right), (1, n - 1 - to_right)):
-            if step > count:
-                continue
-            origin = ring_at(pos - step) if way == 0 else ring_at(pos + step)
-            index = (number * 2 + way) * half + step - 1
-            pltpu.make_async_remote_copy(
-                src_ref=view(origin),
-                dst_ref=view(origin),
-                send_sem=send_sem.at[index],
-                recv_sem=recv_sem.at[index],
-                device_id=(right if way == 0 else left, tp),
-                device_id_type=MESH,
-            ).wait_recv()
-            if step < count:
-                index += 1
-                copy = pltpu.make_async_remote_copy(
-                    src_ref=view(origin),
-                    dst_ref=view(origin),
-                    send_sem=send_sem.at[index],
-                    recv_sem=recv_sem.at[index],
-                    device_id=(right if way == 0 else left, tp),
-                    device_id_type=MESH,
-                )
-                copy.start()
-                started.append(copy)
-
-    send("k", 1)
+        del spread_list[:count]
+
+    def hop_own(k):
+        for part in grain[k]:
+            if k > 0:
+                for which in range(part[0], part[0] + part[1]):
+                    weight_wait("z", k, (which, 1))
+            for kind in ("y", "x", "cz"):
+                start(weight_copy(kind, k, part))
+
+    def hop_side(k):
+        for part in grain[k]:
+            weight_wait("y", k, part)
+            if k % 2 == 0:
+                start(weight_copy("d", k, part))
+            start(weight_copy("cy", k, part))
+            weight_wait("x", k, part)
+            if k % 2 == 1:
+                start(weight_copy("d", k, part))
+            start(weight_copy("cx", k, part))
+
+    def hop_far(k):
+        for part in grain[k]:
+            weight_wait("d", k, part)
+            start(weight_copy("cd", k, part))
+
+    send("k")
     locs["v"].wait()
-    send("v", 1)
+    vbuf[sp] = vraw[...].T
+    send("v")
     locs["g"].wait()
     locs["u"].wait()
 
@@ -311,68 +390,16 @@
 
     lax.fori_loop(0, hidden // 128, transpose, 0)
     locs["d"].wait()
-
-    def units(index):
-        return pl.ds(pl.multiple_of(index * chunk, 16), chunk)
-
     own_piece = pltpu.make_async_copy(
-        wt.at[:, units(sp), :], wall.at[sp, :, units(tp), :], loc_sem.at[5]
+        wt.at[:, pl.ds(pl.multiple_of(z * hq, 16), hq), :], wall.at[sp, :, 0:hq, :], loc_sem.at[5]
     )
     own_piece.start()
-
-    def spread(d):
-        peer = lax.rem(sp + d, n)
-        copy = pltpu.make_async_remote_copy(
-            src_ref=wt.at[:, units(peer), :],
-            dst_ref=wall.at[sp, :, units(tp), :],
-            send_sem=a_send.at[d - 1],
-            recv_sem=a_recv.at[d - 1],
-            device_id=(peer, tp),
-            device_id_type=MESH,
-        )
-        copy.start()
-        started.append(copy)
-
-    across, beside = lax.rem(tp + tn // 2, tn), tp + 1 - 2 * lax.rem(tp, 2)
-
-    def relay(kind, d):
-        slot = lax.rem(sp - d + n, n)
-        owner = across if kind == 2 else tp
-        piece = wall.at[slot, :, units(owner), :]
-        return pltpu.make_async_remote_copy(
-            src_ref=piece,
-            dst_ref=piece,
-            send_sem=w_send.at[kind * n + d],
-            recv_sem=w_recv.at[kind * n + d],
-            device_id=(sp, across if kind == 0 else beside),
-            device_id_type=MESH,
-        )
-
-    def pass_on(d):
-        if d == 0:
-            own_piece.wait()
-        else:
-            slot = lax.rem(sp - d + n, n)
-            piece = wall.at[slot, :, units(tp), :]
-            pltpu.make_async_remote_copy(
-                src_ref=piece,
-                dst_ref=piece,
-                send_sem=a_send.at[d - 1],
-                recv_sem=a_recv.at[d - 1],
-                device_id=(lax.rem(sp + d, n), tp),
-                device_id_type=MESH,
-            ).wait_recv()
-        for kind in (0, 1):
-            copy = relay(kind, d)
-            copy.start()
-            started.append(copy)
-
     spread(1)
-    spread(2)
-    pass_on(0)
+    own_piece.wait()
+    hop_own(0)
 
     for h in range(groups):
-        qs[h] = turned(q_in[:, h * hd : (h + 1) * hd], qg_ref[...])
+        qs[h] = turned(q_in[:, h * hd : (h + 1) * hd], qg_ref[...]).T
     m_s[...] = jnp.full_like(m_s, -1e30)
     l_s[...] = jnp.zeros_like(l_s)
     acc[...] = jnp.zeros_like(acc)
@@ -384,17 +411,15 @@
             slot = slots[0]
             if len(slots) > 1:
                 slot = jnp.where(i < groups, slots[0], slots[1])
-            scores = lax.dot_general(
-                qs[h], kbuf[slot], (((1,), (1,)), ((), ())), preferred_element_type=jnp.float32
-            )
+            scores = jnp.dot(kbuf[slot], qs[h], preferred_element_type=jnp.float32)
             before = m_s[h]
-            highest = jnp.maximum(before, jnp.max(scores, axis=-1, keepdims=True))
+            highest = jnp.maximum(before, jnp.max(scores, axis=0, keepdims=True))
             scale = jnp.exp2((before - highest) * factor)
             probs = jnp.exp2((scores - highest) * factor)
             m_s[h] = highest
-            l_s[h] = l_s[h] * scale + jnp.sum(probs, axis=-1, keepdims=True)
+            l_s[h] = l_s[h] * scale + jnp.sum(probs, axis=0, keepdims=True)
             acc[h] = acc[h] * scale + jnp.dot(
-                probs.astype(jnp.bfloat16), vbuf[slot], preferred_element_type=jnp.float32
+                vbuf[slot], probs.astype(jnp.bfloat16), preferred_element_type=jnp.float32
             )
             return carry
 
@@ -404,19 +429,16 @@
     for step in range(1, half + 1):
         arrive("k", step)
         arrive("v", step)
-        for d in (2 * step + 1, 2 * step + 2):
-            if d < n:
-                spread(d)
+        spread(1 if step < half - 1 else len(spread_list))
+        if step == half - 1:
+            hop_side(0)
         ends = [ring_at(pos - step), ring_at(pos + step)]
         attend(ends if step < half else ends[:1])
-        for d in (2 * step - 5, 2 * step - 4):
-            if 0 < d < n:
-                pass_on(d)
 
     for h in range(groups):
         done = (acc[h] / l_s[h]).astype(jnp.bfloat16)
         for t in range(tn):
-            att[t, :, h * hd : (h + 1) * hd] = done[t * rows : (t + 1) * rows]
+            att[t, :, h * hd : (h + 1) * hd] = done[:, t * rows : (t + 1) * rows].T
     to_heads = []
     for d in range(1, tn):
         peer = lax.rem(tp + d, tn)
@@ -431,8 +453,8 @@
         copy.start()
         to_heads.append(copy)
     heads[tp] = att[tp]
-    for d in range(2 * half - 3, n):
-        pass_on(d)
+    hop_own(1)
+    hop_far(0)
     locs["o"].wait()
     for copy in to_heads:
         copy.wait_recv()
@@ -449,7 +471,7 @@
         proj[:, cols] = total
         return carry
 
-    lax.fori_loop(0, ow.shape[1] // span, project, 0)
+    lax.fori_loop(0, wide // span, project, 0)
     projected = proj[...]
     middle = (
         res_ref[...].astype(jnp.float32)
@@ -458,101 +480,152 @@
     ).astype(jnp.bfloat16)
     mid[...] = middle
     middle = middle.astype(jnp.float32)
-    normed = (
+    toks[pl.ds(pl.multiple_of(z * rows, rows), rows), :] = (
         mg_ref[...] * (middle * lax.rsqrt(jnp.mean(middle * middle, axis=-1, keepdims=True) + EPS))
     ).astype(jnp.bfloat16)
 
-    for way in range(2):
-        toks[way, sp] = normed[way * side : (way + 1) * side]
-
-    def token_copy(way, step):
-        origin = ring_at(pos - (step - 1)) if way == 0 else ring_at(pos + (step - 1))
+    ahead = {0: nz - 1 - z, 1: z}
+    behind = {0: z, 1: nz - 1 - z}
+    next_dev = {0: (lax.rem(sp + 2, n), tp), 1: (lax.rem(sp - 2 + n, n), tp)}
+    side = rows // 2
+
+    def token_copy(way, e, sub, lag):
+        origin = z - (e - lag) if way == 0 else z + (e - lag)
+        part = toks.at[pl.ds(pl.multiple_of(origin * rows + sub * side, 16), side), :]
+        index = (way * nz + e) * 2 + sub
         return pltpu.make_async_remote_copy(
-            src_ref=toks.at[way, origin],
-            dst_ref=toks.at[way, origin],
-            send_sem=t_send.at[way * n + step],
-            recv_sem=t_recv.at[way * n + step],
-            device_id=(right if way == 0 else left, tp),
+            src_ref=part,
+            dst_ref=part,
+            send_sem=t_send.at[index],
+            recv_sem=t_recv.at[index],
+            device_id=next_dev[way],
             device_id_type=MESH,
         )
 
-    def sum_copy(way, step):
-        return pltpu.make_async_remote_copy(
-            src_ref=psend.at[way, step],
-            dst_ref=precv.at[way, step],
-            send_sem=p_send.at[way * n + step],
-            recv_sem=p_recv.at[way * n + step],
-            device_id=(right if way == 0 else left, tp),
-            device_id_type=MESH,
-        )
-
-    for way in range(2):
-        token_copy(way, 1).start()
-    for d in range(n):
-        relay(0, d).wait_recv()
-        copy = relay(2, d)
-        copy.start()
-        started.append(copy)
-    for d in range(n):
-        relay(1, d).wait_recv()
-        relay(2, d).wait_recv()
-
-    def block(step, carry):
+    for sub in range(2):
         for way in range(2):
 
-            @pl.when(step > 0)
+            @pl.when(ahead[way] > 0)
             def _():
-                token_copy(way, step).wait_recv()
-
-            @pl.when(jnp.logical_and(step > 0, step < n - 1))
-            def _():
-                token_copy(way, step + 1).start()
-
-        tokens = jnp.concatenate(
-            [toks[0, ring_at(pos - step)], toks[1, ring_at(pos + step)]], axis=0
-        )
+                token_copy(way, 1, sub, 1).start()
+
+    def token_hop(e):
+        for sub in range(2):
+            for way in range(2):
+
+                @pl.when(behind[way] >= e)
+                def _():
+                    token_copy(way, e, sub, 0).wait_recv()
+
+                    @pl.when(ahead[way] > 0)
+                    def _():
+                        token_copy(way, e + 1, sub, 1).start()
+
+    for k in range(1, nz):
+        if k > 1:
+            hop_own(k)
+        hop_side(k)
+        if k == nz - 1:
+            token_hop(1)
+        hop_far(k)
+    for e in range(2, nz):
+        token_hop(e)
+    for k in range(nz):
+        for part in grain[k]:
+            for kind in ("cz", "cy", "cx", "cd"):
+                weight_wait(kind, k, part)
+
+    def feed(base, size):
         branches = []
         for which in range(2):
-            total = jnp.zeros((rows, hidden // n * tn), jnp.float32)
+            total = jnp.zeros((nz * rows, size), jnp.float32)
             for s in range(n):
                 total += lax.dot_general(
-                    tokens[:, s * depth : (s + 1) * depth],
-                    wall[s, which],
+                    toks[:, s * depth : (s + 1) * depth],
+                    wall[s, which, pl.ds(base, size), :],
                     (((1,), (1,)), ((), ())),
                     preferred_element_type=jnp.float32,
                 )
             branches.append(total)
         gate, up = branches
-        inner = (gate / (1.0 + jnp.exp(-gate)) * up).astype(jnp.bfloat16)
-        for s in range(n):
-            osc[:, s * depth : (s + 1) * depth] = jnp.dot(
-                inner, wall[s, 2], preferred_element_type=jnp.float32
+        return (gate / (1.0 + jnp.exp(-gate)) * up).astype(jnp.bfloat16)
+
+    tile = 256
+
+    def feed_tile(j, carry):
+        base = pl.multiple_of(j * tile, tile)
+        inner[:, pl.ds(base, tile)] = feed(base, tile)
+        return carry
+
+    lax.fori_loop(0, units // tile, feed_tile, 0)
+    rest = units % tile
+    if rest:
+        inner[:, units - rest :] = feed(units - rest, rest)
+
+    blocks = n // 2
+    cut = wide // blocks
+
+    def columns(j):
+        return pl.ds(pl.multiple_of(j * cut, 128), cut)
+
+    def sum_copy(way, d, j):
+        return pltpu.make_async_remote_copy(
+            src_ref=psend.at[way, d - 1, :, columns(j)],
+            dst_ref=precv.at[way, d - 1, :, columns(j)],
+            send_sem=p_send.at[(way * nz + d) * blocks + j],
+            recv_sem=p_recv.at[(way * nz + d) * blocks + j],
+            device_id=next_dev[way],
+            device_id_type=MESH,
+        )
+
+    def sum_wait(way, d, j):
+        sum_copy(way, d + 1, j).wait_recv()
+
+    def share(way, d, j):
+        owner = z + d if way == 0 else z - d
+        return osc[pl.ds(pl.multiple_of(owner * rows, rows), rows), columns(j)]
+
+    def down(j, carry):
+        for part in range(2):
+            s = 2 * j + part
+            osc[:, pl.ds(pl.multiple_of(s * depth, 128), depth)] = jnp.dot(
+                inner[...], wall[s, 2], preferred_element_type=jnp.float32
             )
-
-        @pl.when(step == 0)
-        def _():
-            proj[...] = osc[...]
-
-        @pl.when(step > 0)
-        def _():
+        for way in range(2):
+
+            @pl.when(behind[way] == 0)
+            def _():
+                for d in range(nz - 1, 0, -1):
+                    psend[way, d - 1, :, columns(j)] = share(way, d, j).astype(jnp.bfloat16)
+                    sum_copy(way, d, j).start()
+
+        return carry
+
+    lax.fori_loop(0, blocks, down, 0)
+
+    def collect(j, carry):
+        for d in range(nz - 2, 0, -1):
             for way in range(2):
-                part = slice(way * side, (way + 1) * side)
-
-                @pl.when(step > 1)
+
+                @pl.when(jnp.logical_and(behind[way] > 0, ahead[way] >= d))
                 def _():
-                    sum_copy(way, step - 1).wait_recv()
-                    osc[part] += precv[way, step - 1].astype(jnp.float32)
-
-                psend[way, step] = osc[part].astype(jnp.bfloat16)
-                sum_copy(way, step).start()
+                    sum_wait(way, d, j)
+                    psend[way, d - 1, :, columns(j)] = (
+                        share(way, d, j) + precv[way, d, :, columns(j)].astype(jnp.float32)
+                    ).astype(jnp.bfloat16)
+                    sum_copy(way, d, j).start()
+
+        proj[:, columns(j)] = share(0, 0, j)
+        for way in range(2):
+
+            @pl.when(behind[way] > 0)
+            def _():
+                sum_wait(way, 0, j)
+                proj[:, columns(j)] += precv[way, 0, :, columns(j)].astype(jnp.float32)
 
         return carry
 
-    lax.fori_loop(0, n, block, 0)
-    for way in range(2):
-        sum_copy(way, n - 1).wait_recv()
-        part = slice(way * side, (way + 1) * side)
-        proj[part] += precv[way, n - 1].astype(jnp.float32)
+    lax.fori_loop(0, blocks, collect, 0)
     total = proj[...]
     out_ref[...] = (
         mid[...].astype(jnp.float32)
@@ -561,13 +634,21 @@
     for copy in started + to_heads:
         copy.wait_send()
 
-    def drain(step, carry):
-        for way in range(2):
-            token_copy(way, step).wait_send()
-            sum_copy(way, step).wait_send()
-        return carry
-
-    lax.fori_loop(1, n, drain, 0)
+    for way in range(2):
+        for e in range(1, nz):
+
+            @pl.when(jnp.logical_and(ahead[way] > 0, behind[way] >= e - 1))
+            def _():
+                for sub in range(2):
+                    token_copy(way, e, sub, 1).wait_send()
+
+            @pl.when(ahead[way] >= e)
+            def _():
+                def drain(j, carry):
+                    sum_copy(way, e, j).wait_send()
+                    return carry
+
+                lax.fori_loop(0, blocks, drain, 0)
 
 
 def rotary_tables(tok_rows, head_size):
@@ -600,37 +681,37 @@
         in_specs=[vmem, vmem, hbm, vmem, vmem, vmem, vmem, hbm, vmem, vmem, vmem, hbm, hbm, hbm, vmem],
         out_specs=vmem,
         scratch_shapes=[
-            pltpu.VMEM((groups, tok, hd), b16),
+            pltpu.VMEM((groups, hd, tok), b16),
             pltpu.VMEM((n, tok, hd), b16),
-            pltpu.VMEM((n, tok, hd), b16),
+            pltpu.VMEM((n, hd, tok), b16),
+            pltpu.VMEM((tok, hd), b16),
             pltpu.VMEM((2, depth, hidden), b16),
             pltpu.VMEM((3, hidden, depth), b16),
-            pltpu.VMEM((n, 3, hidden // n * tn, depth), b16),
+            pltpu.VMEM((n, 3, hidden // half * tn, depth), b16),
             pltpu.VMEM((wide, wide), b16),
-            pltpu.VMEM((groups, tok, 1), f32),
-            pltpu.VMEM((groups, tok, 1), f32),
-            pltpu.VMEM((groups, tok, hd), f32),
+            pltpu.VMEM((groups, 1, tok), f32),
+            pltpu.VMEM((groups, 1, tok), f32),
+            pltpu.VMEM((groups, hd, tok), f32),
             pltpu.VMEM((tn, rows, groups * hd), b16),
             pltpu.VMEM((tn, rows, groups * hd), b16),
             pltpu.VMEM((rows, wide), f32),
             pltpu.VMEM((rows, wide), b16),
-            pltpu.VMEM((2, n, rows // 2, wide), b16),
-            pltpu.VMEM((rows, wide), f32),
-            pltpu.VMEM((2, n, rows // 2, wide), b16),
-            pltpu.VMEM((2, n, rows // 2, wide), b16),
+            pltpu.VMEM((half * rows, wide), b16),
+            pltpu.VMEM((half * rows, hidden // half * tn), b16),
+            pltpu.VMEM((half * rows, wide), f32),
+            pltpu.VMEM((2, half - 1, rows, wide), b16),
+            pltpu.VMEM((2, half - 1, rows, wide), b16),
             pltpu.SemaphoreType.DMA((6,)),
             pltpu.SemaphoreType.DMA((4 * half,)),
             pltpu.SemaphoreType.DMA((4 * half,)),
             pltpu.SemaphoreType.DMA((tn - 1,)),
             pltpu.SemaphoreType.DMA((tn - 1,)),
-            pltpu.SemaphoreType.DMA((n - 1,)),
-            pltpu.SemaphoreType.DMA((n - 1,)),
-            pltpu.SemaphoreType.DMA((3 * n,)),
-            pltpu.SemaphoreType.DMA((3 * n,)),
-            pltpu.SemaphoreType.DMA((2 * n,)),
-            pltpu.SemaphoreType.DMA((2 * n,)),
-            pltpu.SemaphoreType.DMA((2 * n,)),
-            pltpu.SemaphoreType.DMA((2 * n,)),
+            pltpu.SemaphoreType.DMA((8 * half * 3,)),
+            pltpu.SemaphoreType.DMA((8 * half * 3,)),
+            pltpu.SemaphoreType.DMA((2 * half * 2,)),
+            pltpu.SemaphoreType.DMA((2 * half * 2,)),
+            pltpu.SemaphoreType.DMA((2 * half * half,)),
+            pltpu.SemaphoreType.DMA((2 * half * half,)),
         ],
         compiler_params=pltpu.CompilerParams(
             collective_id=0, has_side_effects=True, vmem_limit_bytes=67043328
@@ -659,7 +740,7 @@
     tok, hd = args[1].shape
     depth, hidden = args[9].shape
     fits = n % 2 == 0 and 4 <= n <= 8 and depth % 128 == 0 and hidden % 128 == 0
-    fits = fits and tn == 4 and hidden % (16 * n) == 0 and args[7].shape[0] % 32 == 0
+    fits = fits and tn == 4 and hidden % (8 * n) == 0 and args[7].shape[0] % 128 == 0
     if fits and tok % 256 == 0 and hd == 128:
         return fused(n, tn, *args)
     return on_device(*args)

time: 215 us -> 192 us (0.89); the launches traced: 212 us -> 191 us
  Pallas kernels: 208 us -> 187 us
    pallas_call x1, Pallas kernels: 208 us -> 187 us  [fused(): pl.pallas_call(functools.partial(layer_kernel, n, tn), out_shape=jax.Shap...]
where the time goes in v1:
time: 192 us; the launch traced here: 191 us
  Pallas kernels  187 us (97%)
    pallas_call x1, Pallas kernels, fused(): pl.pallas_call(functools.partial(layer_kernel, n, tn), out_shape=jax.Shap...  187 us

profile of v1, /device:TPU:0, one launch (start us, length us, event | category | flops | bytes accessed | tf_op | source)
XLA Modules:
  0.0 191.2 jit_solution(7608830907182471347)
XLA Ops:
  0.0 1.9 negate_select_fusion
  1.9 187.4 %shard_map.127 = bf16[128,2048]{1,0:T(8,128)(2,1)} custom-call(bf16[512,512]{1,0:T(8,128)(2,1)} %q_in.1, bf16[512,128]{1,0:T(8,128)(2,1)} %k_in.1, bf16[512,128]{1,0:T(8,128)(2,1)} %v_hbm.1, f32[512,128]{1,0:T(8,128)} %get-tuple-element.6.cos_ref, f32[512,128]{1,0:T(8,128)} %get-tuple-element.5.sin_ref, f32[1,128]{1,0:T(1,128)} %bitcast.8, ...), custom_call_target="tpu_custom_call" | custom-call | tf_op jit(solution)/shard_map/pallas_call | solution.py:678
  189.3 1.9 copy.15
  (3 shorter events, 0.0 us)

commit v2 on v1

--- a/solution.py
+++ b/solution.py
@@ -141,8 +141,8 @@
     q_in,
     k_in,
     v_hbm,
-    cos_ref,
-    sin_ref,
+    cos_in,
+    sin_in,
     qg_ref,
     kg_ref,
     ow_hbm,
@@ -154,6 +154,8 @@
     down_hbm,
     fg_ref,
     out_ref,
+    cos_ref,
+    sin_ref,
     qs,
     kbuf,
     vbuf,
@@ -211,6 +213,16 @@
     hq = hidden // nz
     units = hq * tn
 
+    barrier = pltpu.get_barrier_semaphore()
+    for d in range(1, n):
+        pl.semaphore_signal(
+            barrier, inc=1, device_id=(lax.rem(sp + d, n), tp), device_id_type=MESH
+        )
+    for d in range(1, tn):
+        pl.semaphore_signal(
+            barrier, inc=1, device_id=(sp, lax.rem(tp + d, tn)), device_id_type=MESH
+        )
+
     locs = {
         "v": pltpu.make_async_copy(v_hbm, vraw, loc_sem.at[0]),
         "g": pltpu.make_async_copy(gate_hbm, raw.at[0], loc_sem.at[1]),
@@ -231,17 +243,14 @@
         other = jnp.where(first, pltpu.roll(x, hd - quarter, 1), pltpu.roll(x, quarter, 1))
         return (x * cos_ref[...] + other * sin_ref[...]).astype(jnp.bfloat16)
 
+    low = lane[:GRID_W] < 2 * quarter
+    grid_rows = tok // GRID_W
+    for row in range(grid_rows):
+        part = slice(row * GRID_W, (row + 1) * GRID_W)
+        for small, large in ((cos_in, cos_ref), (sin_in, sin_ref)):
+            large[part, :] = jnp.where(low, small[row : row + 1, :], small[grid_rows:, :])
     kbuf[sp] = turned(k_in[...], kg_ref[...])
 
-    barrier = pltpu.get_barrier_semaphore()
-    for d in range(1, n):
-        pl.semaphore_signal(
-            barrier, inc=1, device_id=(lax.rem(sp + d, n), tp), device_id_type=MESH
-        )
-    for d in range(1, tn):
-        pl.semaphore_signal(
-            barrier, inc=1, device_id=(sp, lax.rem(tp + d, tn)), device_id_type=MESH
-        )
     pl.semaphore_wait(barrier, n - 1 + tn - 1)
 
     started = []
@@ -285,8 +294,11 @@
                 start(ring_copy(name, way, step + 1, origin))
 
     bases = {"z": 0, "x": 1, "y": 2, "d": 3, "cz": 4, "cy": 5, "cx": 6, "cd": 7}
-    grain = {k: [(0, 3)] for k in range(nz)}
-    grain[nz - 1] = [(0, 1), (1, 1), (2, 1)]
+    whole = [(0, 3)]
+    thirds = [(0, 1), (1, 1), (2, 1)]
+
+    def parts(kind, k):
+        return thirds if k == nz - 1 or kind == "z" or (k == 0 and kind in ("y", "d")) else whole
 
     def column(k, side):
         return 2 * lax.rem(z + k, nz) + side
@@ -318,18 +330,21 @@
         )
 
     def weight_wait(kind, k, part):
-        index = (bases[kind] * nz + k) * 3 + part[0]
         side = y if kind in ("z", "x", "cz", "cx") else other_y
         r = {"z": 0, "y": 0, "x": 2, "d": 2, "cz": 1, "cy": 1, "cx": 3, "cd": 3}[kind]
-        here = piece(column(k, side), r, part)
-        pltpu.make_async_remote_copy(
-            src_ref=here,
-            dst_ref=here,
-            send_sem=w_send.at[index],
-            recv_sem=w_recv.at[index],
-            device_id=c_dev,
-            device_id_type=MESH,
-        ).wait_recv()
+        for small in parts(kind, k):
+            if small[0] < part[0] or small[0] >= part[0] + part[1]:
+                continue
+            index = (bases[kind] * nz + k) * 3 + small[0]
+            here = piece(column(k, side), r, small)
+            pltpu.make_async_remote_copy(
+                src_ref=here,
+                dst_ref=here,
+                send_sem=w_send.at[index],
+                recv_sem=w_recv.at[index],
+                device_id=c_dev,
+                device_id_type=MESH,
+            ).wait_recv()
 
     spread_list = [(k, which) for k in range(1, nz) for which in range(3)]
 
@@ -351,27 +366,23 @@
             )
         del spread_list[:count]
 
-    def hop_own(k):
-        for part in grain[k]:
+    def hop_own(k, kinds=("y", "x", "cz")):
+        for part in thirds if k == nz - 1 else whole:
             if k > 0:
-                for which in range(part[0], part[0] + part[1]):
-                    weight_wait("z", k, (which, 1))
-            for kind in ("y", "x", "cz"):
+                weight_wait("z", k, part)
+            for kind in kinds:
                 start(weight_copy(kind, k, part))
 
     def hop_side(k):
-        for part in grain[k]:
-            weight_wait("y", k, part)
-            if k % 2 == 0:
-                start(weight_copy("d", k, part))
-            start(weight_copy("cy", k, part))
-            weight_wait("x", k, part)
-            if k % 2 == 1:
-                start(weight_copy("d", k, part))
-            start(weight_copy("cx", k, part))
+        for part in thirds if k == nz - 1 else whole:
+            for kind, odd in (("y", 0), ("x", 1)):
+                weight_wait(kind, k, part)
+                if k % 2 == odd:
+                    start(weight_copy("d", k, part))
+                start(weight_copy("c" + kind, k, part))
 
     def hop_far(k):
-        for part in grain[k]:
+        for part in thirds if k == nz - 1 else whole:
             weight_wait("d", k, part)
             start(weight_copy("cd", k, part))
 
@@ -396,7 +407,8 @@
     own_piece.start()
     spread(1)
     own_piece.wait()
-    hop_own(0)
+    hop_own(0, ("x", "cz"))
+    start(weight_copy("y", 0, thirds[0]))
 
     for h in range(groups):
         qs[h] = turned(q_in[:, h * hd : (h + 1) * hd], qg_ref[...]).T
@@ -407,31 +419,39 @@
 
     def attend(slots):
         def one(i, carry):
-            h = lax.rem(i, groups)
             slot = slots[0]
             if len(slots) > 1:
-                slot = jnp.where(i < groups, slots[0], slots[1])
-            scores = jnp.dot(kbuf[slot], qs[h], preferred_element_type=jnp.float32)
-            before = m_s[h]
-            highest = jnp.maximum(before, jnp.max(scores, axis=0, keepdims=True))
-            scale = jnp.exp2((before - highest) * factor)
-            probs = jnp.exp2((scores - highest) * factor)
-            m_s[h] = highest
-            l_s[h] = l_s[h] * scale + jnp.sum(probs, axis=0, keepdims=True)
-            acc[h] = acc[h] * scale + jnp.dot(
-                vbuf[slot], probs.astype(jnp.bfloat16), preferred_element_type=jnp.float32
-            )
+                slot = jnp.where(i == 0, slots[0], slots[1])
+            for h in range(groups):
+                scores = jnp.dot(kbuf[slot], qs[h], preferred_element_type=jnp.float32)
+                before = m_s[h]
+                highest = jnp.maximum(before, jnp.max(scores, axis=0, keepdims=True))
+                scale = jnp.exp2((before - highest) * factor)
+                probs = jnp.exp2((scores - highest) * factor)
+                m_s[h] = highest
+                l_s[h] = l_s[h] * scale + jnp.sum(probs, axis=0, keepdims=True)
+                acc[h] = acc[h] * scale + jnp.dot(
+                    vbuf[slot], probs.astype(jnp.bfloat16), preferred_element_type=jnp.float32
+                )
             return carry
 
-        lax.fori_loop(0, groups * len(slots), one, 0)
+        lax.fori_loop(0, len(slots), one, 0)
 
     attend([sp])
     for step in range(1, half + 1):
         arrive("k", step)
         arrive("v", step)
         spread(1 if step < half - 1 else len(spread_list))
+        if step < 3:
+            start(weight_copy("y", 0, thirds[step]))
+        if step <= 3:
+            weight_wait("y", 0, thirds[step - 1])
+            start(weight_copy("d", 0, thirds[step - 1]))
         if step == half - 1:
-            hop_side(0)
+            start(weight_copy("cy", 0, whole[0]))
+            weight_wait("x", 0, whole[0])
+            start(weight_copy("cx", 0, whole[0]))
+            hop_own(1)
         ends = [ring_at(pos - step), ring_at(pos + step)]
         attend(ends if step < half else ends[:1])
 
@@ -453,8 +473,8 @@
         copy.start()
         to_heads.append(copy)
     heads[tp] = att[tp]
-    hop_own(1)
     hop_far(0)
+    hop_side(1)
     locs["o"].wait()
     for copy in to_heads:
         copy.wait_recv()
@@ -480,7 +500,7 @@
     ).astype(jnp.bfloat16)
     mid[...] = middle
     middle = middle.astype(jnp.float32)
-    toks[pl.ds(pl.multiple_of(z * rows, rows), rows), :] = (
+    normed = (
         mg_ref[...] * (middle * lax.rsqrt(jnp.mean(middle * middle, axis=-1, keepdims=True) + EPS))
     ).astype(jnp.bfloat16)
 
@@ -489,176 +509,197 @@
     next_dev = {0: (lax.rem(sp + 2, n), tp), 1: (lax.rem(sp - 2 + n, n), tp)}
     side = rows // 2
 
-    def token_copy(way, e, sub, lag):
+    def line_rows(at):
+        return pl.ds(pl.multiple_of(at * side, 16), side)
+
+    def token_copy(part, way, e, lag):
         origin = z - (e - lag) if way == 0 else z + (e - lag)
-        part = toks.at[pl.ds(pl.multiple_of(origin * rows + sub * side, 16), side), :]
-        index = (way * nz + e) * 2 + sub
+        block = toks.at[part, line_rows(origin), :]
+        index = (part * 2 + way) * nz + e
         return pltpu.make_async_remote_copy(
-            src_ref=part,
-            dst_ref=part,
+            src_ref=block,
+            dst_ref=block,
             send_sem=t_send.at[index],
             recv_sem=t_recv.at[index],
             device_id=next_dev[way],
             device_id_type=MESH,
         )
 
-    for sub in range(2):
+    for part in range(2):
+        toks[part, line_rows(z), :] = normed[part * side : (part + 1) * side]
+    for part in range(2):
         for way in range(2):
 
             @pl.when(ahead[way] > 0)
             def _():
-                token_copy(way, 1, sub, 1).start()
-
-    def token_hop(e):
-        for sub in range(2):
-            for way in range(2):
-
-                @pl.when(behind[way] >= e)
+                token_copy(part, way, 1, 1).start()
+
+    def token_hop(part, e):
+        for way in range(2):
+
+            @pl.when(behind[way] >= e)
+            def _():
+                token_copy(part, way, e, 0).wait_recv()
+
+                @pl.when(ahead[way] > 0)
                 def _():
-                    token_copy(way, e, sub, 0).wait_recv()
-
-                    @pl.when(ahead[way] > 0)
-                    def _():
-                        token_copy(way, e + 1, sub, 1).start()
-
-    for k in range(1, nz):
-        if k > 1:
-            hop_own(k)
-        hop_side(k)
-        if k == nz - 1:
-            token_hop(1)
-        hop_far(k)
-    for e in range(2, nz):
-        token_hop(e)
-    for k in range(nz):
-        for part in grain[k]:
+                    token_copy(part, way, e + 1, 1).start()
+
+    def weights_in():
+        for k in range(nz):
             for kind in ("cz", "cy", "cx", "cd"):
-                weight_wait(kind, k, part)
-
-    def feed(base, size):
-        branches = []
-        for which in range(2):
-            total = jnp.zeros((nz * rows, size), jnp.float32)
-            for s in range(n):
-                total += lax.dot_general(
-                    toks[:, s * depth : (s + 1) * depth],
-                    wall[s, which, pl.ds(base, size), :],
-                    (((1,), (1,)), ((), ())),
-                    preferred_element_type=jnp.float32,
-                )
-            branches.append(total)
-        gate, up = branches
-        return (gate / (1.0 + jnp.exp(-gate)) * up).astype(jnp.bfloat16)
-
-    tile = 256
-
-    def feed_tile(j, carry):
-        base = pl.multiple_of(j * tile, tile)
-        inner[:, pl.ds(base, tile)] = feed(base, tile)
-        return carry
-
-    lax.fori_loop(0, units // tile, feed_tile, 0)
-    rest = units % tile
-    if rest:
-        inner[:, units - rest :] = feed(units - rest, rest)
-
-    blocks = n // 2
+                weight_wait(kind, k, (0, 3))
+
+    def feed(part):
+        def feed_tile(r, carry):
+            base = pl.multiple_of(r * hq, 16)
+            branches = []
+            for which in range(2):
+                total = jnp.zeros((hq, nz * side), jnp.float32)
+                for s in range(n):
+                    total += lax.dot_general(
+                        wall[s, which, pl.ds(base, hq), :],
+                        toks[part, :, s * depth : (s + 1) * depth],
+                        (((1,), (1,)), ((), ())),
+                        preferred_element_type=jnp.float32,
+                    )
+                branches.append(total)
+            gate, up = branches
+            inner[pl.ds(base, hq), :] = (gate / (1.0 + jnp.exp(-gate)) * up).astype(jnp.bfloat16)
+            return carry
+
+        lax.fori_loop(0, tn, feed_tile, 0)
+
+    blocks = 2
     cut = wide // blocks
 
     def columns(j):
         return pl.ds(pl.multiple_of(j * cut, 128), cut)
 
-    def sum_copy(way, d, j):
+    def sum_copy(part, way, d, j):
+        index = ((part * 2 + way) * nz + d) * blocks + j
         return pltpu.make_async_remote_copy(
-            src_ref=psend.at[way, d - 1, :, columns(j)],
-            dst_ref=precv.at[way, d - 1, :, columns(j)],
-            send_sem=p_send.at[(way * nz + d) * blocks + j],
-            recv_sem=p_recv.at[(way * nz + d) * blocks + j],
+            src_ref=psend.at[part, way, d - 1, :, columns(j)],
+            dst_ref=precv.at[part, way, d - 1, :, columns(j)],
+            send_sem=p_send.at[index],
+            recv_sem=p_recv.at[index],
             device_id=next_dev[way],
             device_id_type=MESH,
         )
 
-    def sum_wait(way, d, j):
-        sum_copy(way, d + 1, j).wait_recv()
-
-    def share(way, d, j):
+    def sum_wait(part, way, d, j):
+        sum_copy(part, way, d + 1, j).wait_recv()
+
+    def share(part, way, d, j):
         owner = z + d if way == 0 else z - d
-        return osc[pl.ds(pl.multiple_of(owner * rows, rows), rows), columns(j)]
-
-    def down(j, carry):
-        for part in range(2):
-            s = 2 * j + part
-            osc[:, pl.ds(pl.multiple_of(s * depth, 128), depth)] = jnp.dot(
-                inner[...], wall[s, 2], preferred_element_type=jnp.float32
-            )
-        for way in range(2):
-
-            @pl.when(behind[way] == 0)
-            def _():
-                for d in range(nz - 1, 0, -1):
-                    psend[way, d - 1, :, columns(j)] = share(way, d, j).astype(jnp.bfloat16)
-                    sum_copy(way, d, j).start()
-
-        return carry
-
-    lax.fori_loop(0, blocks, down, 0)
-
-    def collect(j, carry):
-        for d in range(nz - 2, 0, -1):
+        return osc[part, line_rows(owner), columns(j)]
+
+    def down(part):
+        def down_block(j, carry):
+            for which in range(cut // depth):
+                s = (cut // depth) * j + which
+                osc[part, :, pl.ds(pl.multiple_of(s * depth, 128), depth)] = lax.dot_general(
+                    inner[...],
+                    wall[s, 2],
+                    (((0,), (0,)), ((), ())),
+                    preferred_element_type=jnp.float32,
+                )
             for way in range(2):
 
-                @pl.when(jnp.logical_and(behind[way] > 0, ahead[way] >= d))
+                @pl.when(behind[way] == 0)
                 def _():
-                    sum_wait(way, d, j)
-                    psend[way, d - 1, :, columns(j)] = (
-                        share(way, d, j) + precv[way, d, :, columns(j)].astype(jnp.float32)
-                    ).astype(jnp.bfloat16)
-                    sum_copy(way, d, j).start()
-
-        proj[:, columns(j)] = share(0, 0, j)
-        for way in range(2):
-
-            @pl.when(behind[way] > 0)
-            def _():
-                sum_wait(way, 0, j)
-                proj[:, columns(j)] += precv[way, 0, :, columns(j)].astype(jnp.float32)
-
-        return carry
-
-    lax.fori_loop(0, blocks, collect, 0)
-    total = proj[...]
-    out_ref[...] = (
-        mid[...].astype(jnp.float32)
-        + fg_ref[...] * (total * lax.rsqrt(jnp.mean(total * total, axis=-1, keepdims=True) + EPS))
-    ).astype(jnp.bfloat16)
+                    for d in range(nz - 1, 0, -1):
+                        psend[part, way, d - 1, :, columns(j)] = share(part, way, d, j).astype(
+                            jnp.bfloat16
+                        )
+                        sum_copy(part, way, d, j).start()
+
+            return carry
+
+        lax.fori_loop(0, blocks, down_block, 0)
+
+    def collect(part):
+        mine = slice(part * side, (part + 1) * side)
+
+        def collect_block(j, carry):
+            for d in range(nz - 2, 0, -1):
+                for way in range(2):
+
+                    @pl.when(jnp.logical_and(behind[way] > 0, ahead[way] >= d))
+                    def _():
+                        sum_wait(part, way, d, j)
+                        psend[part, way, d - 1, :, columns(j)] = (
+                            share(part, way, d, j)
+                            + precv[part, way, d, :, columns(j)].astype(jnp.float32)
+                        ).astype(jnp.bfloat16)
+                        sum_copy(part, way, d, j).start()
+
+            proj[mine, columns(j)] = share(part, 0, 0, j)
+            for way in range(2):
+
+                @pl.when(behind[way] > 0)
+                def _():
+                    sum_wait(part, way, 0, j)
+                    proj[mine, columns(j)] += precv[part, way, 0, :, columns(j)].astype(jnp.float32)
+
+            return carry
+
+        lax.fori_loop(0, blocks, collect_block, 0)
+        total = proj[mine]
+        out_ref[mine] = (
+            mid[mine].astype(jnp.float32)
+            + fg_ref[...] * (total * lax.rsqrt(jnp.mean(total * total, axis=-1, keepdims=True) + EPS))
+        ).astype(jnp.bfloat16)
+
+    hop_far(1)
+    hop_own(2)
+    token_hop(0, 1)
+    hop_own(3)
+    hop_side(2)
+    token_hop(1, 1)
+    token_hop(0, 2)
+    hop_side(3)
+    token_hop(1, 2)
+    token_hop(0, 3)
+    hop_far(2)
+    hop_far(3)
+    weights_in()
+    feed(0)
+    down(0)
+    token_hop(1, 3)
+    feed(1)
+    down(1)
+    collect(0)
+    collect(1)
     for copy in started + to_heads:
         copy.wait_send()
 
-    for way in range(2):
-        for e in range(1, nz):
-
-            @pl.when(jnp.logical_and(ahead[way] > 0, behind[way] >= e - 1))
-            def _():
-                for sub in range(2):
-                    token_copy(way, e, sub, 1).wait_send()
-
-            @pl.when(ahead[way] >= e)
-            def _():
-                def drain(j, carry):
-                    sum_copy(way, e, j).wait_send()
-                    return carry
-
-                lax.fori_loop(0, blocks, drain, 0)
+    for part in range(2):
+        for way in range(2):
+            for e in range(1, nz):
+
+                @pl.when(jnp.logical_and(ahead[way] > 0, behind[way] >= e - 1))
+                def _():
+                    token_copy(part, way, e, 1).wait_send()
+
+                @pl.when(ahead[way] >= e)
+                def _():
+                    def drain(j, carry):
+                        sum_copy(part, way, e, j).wait_send()
+                        return carry
+
+                    lax.fori_loop(0, blocks, drain, 0)
 
 
 def rotary_tables(tok_rows, head_size):
     quarter = head_size // 4
-    positions = lax.axis_index("sp") * tok_rows + jnp.arange(tok_rows, dtype=jnp.int32)
+    grid_rows = tok_rows // GRID_W
     lane = jnp.arange(head_size, dtype=jnp.int32)
     freqs = 10000.0 ** (-(lane % quarter).astype(jnp.float32) / quarter)
-    row = (positions // GRID_W).astype(jnp.float32)[:, None]
-    column = (positions % GRID_W).astype(jnp.float32)[:, None]
-    angle = jnp.where(lane < 2 * quarter, row, column) * freqs
+    index = jnp.arange(grid_rows + GRID_W, dtype=jnp.int32)
+    base = lax.axis_index("sp") * grid_rows
+    place = jnp.where(index < grid_rows, base + index, index - grid_rows)
+    angle = place.astype(jnp.float32)[:, None] * freqs
     sine = jnp.sin(angle)
     return jnp.cos(angle), jnp.where(lane % (2 * quarter) < quarter, -sine, sine)
 
@@ -681,6 +722,8 @@
         in_specs=[vmem, vmem, hbm, vmem, vmem, vmem, vmem, hbm, vmem, vmem, vmem, hbm, hbm, hbm, vmem],
         out_specs=vmem,
         scratch_shapes=[
+            pltpu.VMEM((tok, hd), f32),
+            pltpu.VMEM((tok, hd), f32),
             pltpu.VMEM((groups, hd, tok), b16),
             pltpu.VMEM((n, tok, hd), b16),
             pltpu.VMEM((n, hd, tok), b16),
@@ -696,11 +739,11 @@
             pltpu.VMEM((tn, rows, groups * hd), b16),
             pltpu.VMEM((rows, wide), f32),
             pltpu.VMEM((rows, wide), b16),
-            pltpu.VMEM((half * rows, wide), b16),
-            pltpu.VMEM((half * rows, hidden // half * tn), b16),
-            pltpu.VMEM((half * rows, wide), f32),
-            pltpu.VMEM((2, half - 1, rows, wide), b16),
-            pltpu.VMEM((2, half - 1, rows, wide), b16),
+            pltpu.VMEM((2, half * rows // 2, wide), b16),
+            pltpu.VMEM((hidden // half * tn, half * rows // 2), b16),
+            pltpu.VMEM((2, half * rows // 2, wide), f32),
+            pltpu.VMEM((2, 2, half - 1, rows // 2, wide), b16),
+            pltpu.VMEM((2, 2, half - 1, rows // 2, wide), b16),
             pltpu.SemaphoreType.DMA((6,)),
             pltpu.SemaphoreType.DMA((4 * half,)),
             pltpu.SemaphoreType.DMA((4 * half,)),
@@ -710,8 +753,8 @@
             pltpu.SemaphoreType.DMA((8 * half * 3,)),
             pltpu.SemaphoreType.DMA((2 * half * 2,)),
             pltpu.SemaphoreType.DMA((2 * half * 2,)),
-            pltpu.SemaphoreType.DMA((2 * half * half,)),
-            pltpu.SemaphoreType.DMA((2 * half * half,)),
+            pltpu.SemaphoreType.DMA((8 * half,)),
+            pltpu.SemaphoreType.DMA((8 * half,)),
         ],
         compiler_params=pltpu.CompilerParams(
             collective_id=0, has_side_effects=True, vmem_limit_bytes=67043328
@@ -739,7 +782,7 @@
     n, tn = mesh.shape["sp"], mesh.shape["tp"]
     tok, hd = args[1].shape
     depth, hidden = args[9].shape
-    fits = n % 2 == 0 and 4 <= n <= 8 and depth % 128 == 0 and hidden % 128 == 0
+    fits = n % 2 == 0 and n == 8 and depth % 128 == 0 and hidden % 128 == 0
     fits = fits and tn == 4 and hidden % (8 * n) == 0 and args[7].shape[0] % 128 == 0
     if fits and tok % 256 == 0 and hd == 128:
         return fused(n, tn, *args)

time: 192 us -> 166 us (0.86); the launches traced: 191 us -> 163 us
  Pallas kernels: 187 us -> 160 us
    pallas_call x1, Pallas kernels: 187 us -> 160 us  [fused(): pl.pallas_call(functools.partial(layer_kernel, n, tn), out_shape=jax.Shap...]
where the time goes in v2:
time: 166 us; the launch traced here: 163 us
  Pallas kernels  160 us (96%)
  local copies, waits for them, and re-layouts  1.88 us (1%)
    pallas_call x1, Pallas kernels, fused(): pl.pallas_call(functools.partial(layer_kernel, n, tn), out_shape=jax.Shap...  160 us

profile of v2, /device:TPU:0, one launch (start us, length us, event | category | flops | bytes accessed | tf_op | source)
XLA Modules:
  0.0 162.8 jit_solution(12897476090977813940)
XLA Ops:
  0.0 0.8 negate_select_fusion
  0.9 160.1 %shard_map.127 = bf16[128,2048]{1,0:T(8,128)(2,1)} custom-call(bf16[512,512]{1,0:T(8,128)(2,1)} %q_in.1, bf16[512,128]{1,0:T(8,128)(2,1)} %k_in.1, bf16[512,128]{1,0:T(8,128)(2,1)} %v_hbm.1, f32[72,128]{1,0:T(8,128)} %get-tuple-element.6.cos_in, f32[72,128]{1,0:T(8,128)} %get-tuple-element.5.sin_in, f32[1,128]{1,0:T(1,128)} %bitcast.8, f32[1,128]{1,0:T(1,128)} %bitcast.9, ...), custom_call_target="tpu_custom_call" | custom-call | tf_op jit(solution)/shard_map/pallas_call | solution.py:719
  160.9 1.9 %copy.15 = bf16[128,2048]{1,0:T(8,128)(2,1)} copy(bf16[128,2048]{1,0:T(8,128)(2,1)} %shard_map.127) | data formatting | bytes 1048576
  (3 shorter events, 0.0 us)

commit v3 on v2

--- a/solution.py
+++ b/solution.py
@@ -153,6 +153,7 @@
     up_hbm,
     down_hbm,
     fg_ref,
+    out_hbm,
     out_ref,
     cos_ref,
     sin_ref,
@@ -298,7 +299,10 @@
     thirds = [(0, 1), (1, 1), (2, 1)]
 
     def parts(kind, k):
-        return thirds if k == nz - 1 or kind == "z" or (k == 0 and kind in ("y", "d")) else whole
+        return thirds if k > 0 or kind in ("y", "d") else whole
+
+    def diagonal(k, which):
+        return "x" if k == 0 or (k > 1 and which != 1) else "y"
 
     def column(k, side):
         return 2 * lax.rem(z + k, nz) + side
@@ -312,7 +316,7 @@
             slot, r_from, r_to, dev = column(k, y), 0, 2, x_dev
         elif kind == "y":
             slot, r_from, r_to, dev = column(k, y), 0, 0, y_dev
-        elif kind == "d" and k % 2 == 0:
+        elif kind == "d" and diagonal(k, part[0]) == "x":
             slot, r_from, r_to, dev = column(k, other_y), 0, 2, x_dev
         elif kind == "d":
             slot, r_from, r_to, dev = column(k, y), 2, 2, y_dev
@@ -346,7 +350,7 @@
                 device_id_type=MESH,
             ).wait_recv()
 
-    spread_list = [(k, which) for k in range(1, nz) for which in range(3)]
+    spread_list = [(k, which) for k in (1, 3, 2) for which in range(3)]
 
     def spread(count):
         for k, which in spread_list[:count]:
@@ -366,25 +370,27 @@
             )
         del spread_list[:count]
 
-    def hop_own(k, kinds=("y", "x", "cz")):
-        for part in thirds if k == nz - 1 else whole:
+    def hop_own(k, some=(0, 1, 2)):
+        for which in some:
+            weight_wait("z", k, thirds[which])
+            for kind in ("y", "x", "cz"):
+                start(weight_copy(kind, k, thirds[which]))
+
+    def hop_side(k, some=(0, 1, 2)):
+        for which in some:
+            for kind, route in (("y", "x"), ("x", "y")):
+                weight_wait(kind, k, thirds[which])
+                if diagonal(k, which) == route:
+                    start(weight_copy("d", k, thirds[which]))
+                start(weight_copy("c" + kind, k, thirds[which]))
+
+    def hop_far(k, some=(0, 1, 2)):
+        for which in some:
+            weight_wait("d", k, thirds[which])
             if k > 0:
-                weight_wait("z", k, part)
-            for kind in kinds:
-                start(weight_copy(kind, k, part))
-
-    def hop_side(k):
-        for part in thirds if k == nz - 1 else whole:
-            for kind, odd in (("y", 0), ("x", 1)):
-                weight_wait(kind, k, part)
-                if k % 2 == odd:
-                    start(weight_copy("d", k, part))
-                start(weight_copy("c" + kind, k, part))
-
-    def hop_far(k):
-        for part in thirds if k == nz - 1 else whole:
-            weight_wait("d", k, part)
-            start(weight_copy("cd", k, part))
+                start(weight_copy("cd", k, thirds[which]))
+        if k == 0:
+            start(weight_copy("cd", k, whole[0]))
 
     send("k")
     locs["v"].wait()
@@ -407,7 +413,8 @@
     own_piece.start()
     spread(1)
     own_piece.wait()
-    hop_own(0, ("x", "cz"))
+    start(weight_copy("x", 0, whole[0]))
+    start(weight_copy("cz", 0, whole[0]))
     start(weight_copy("y", 0, thirds[0]))
 
     for h in range(groups):
@@ -441,7 +448,8 @@
     for step in range(1, half + 1):
         arrive("k", step)
         arrive("v", step)
-        spread(1 if step < half - 1 else len(spread_list))
+        if step != half - 1:
+            spread(1 if step < half else 4)
         if step < 3:
             start(weight_copy("y", 0, thirds[step]))
         if step <= 3:
@@ -475,6 +483,7 @@
     heads[tp] = att[tp]
     hop_far(0)
     hop_side(1)
+    hop_own(3, (0, 1))
     locs["o"].wait()
     for copy in to_heads:
         copy.wait_recv()
@@ -527,23 +536,30 @@
 
     for part in range(2):
         toks[part, line_rows(z), :] = normed[part * side : (part + 1) * side]
-    for part in range(2):
+    def token_send(part):
         for way in range(2):
 
             @pl.when(ahead[way] > 0)
             def _():
                 token_copy(part, way, 1, 1).start()
 
+    token_send(0)
+
     def token_hop(part, e):
         for way in range(2):
 
-            @pl.when(behind[way] >= e)
+            @pl.when(jnp.logical_and(behind[way] >= e, ahead[way] > 0))
             def _():
                 token_copy(part, way, e, 0).wait_recv()
-
-                @pl.when(ahead[way] > 0)
-                def _():
-                    token_copy(part, way, e + 1, 1).start()
+                token_copy(part, way, e + 1, 1).start()
+
+    def tokens_in(part):
+        for way in range(2):
+
+            @pl.when(ahead[way] == 0)
+            def _():
+                for e in range(1, nz):
+                    token_copy(part, way, e, 0).wait_recv()
 
     def weights_in():
         for k in range(nz):
@@ -570,7 +586,7 @@
 
         lax.fori_loop(0, tn, feed_tile, 0)
 
-    blocks = 2
+    blocks = 1
     cut = wide // blocks
 
     def columns(j):
@@ -650,23 +666,31 @@
             mid[mine].astype(jnp.float32)
             + fg_ref[...] * (total * lax.rsqrt(jnp.mean(total * total, axis=-1, keepdims=True) + EPS))
         ).astype(jnp.bfloat16)
-
+        result(part).start()
+
+    def result(part):
+        mine = pl.ds(part * side, side)
+        return pltpu.make_async_copy(out_ref.at[mine], out_hbm.at[mine], loc_sem.at[6 + part])
+
+    spread(2)
+    hop_own(3, (2,))
     hop_far(1)
+    token_hop(0, 1)
+    hop_side(3)
     hop_own(2)
-    token_hop(0, 1)
-    hop_own(3)
-    hop_side(2)
+    token_hop(0, 2)
+    hop_side(2, (0,))
+    token_send(1)
+    hop_side(2, (1, 2))
+    hop_far(3)
     token_hop(1, 1)
-    token_hop(0, 2)
-    hop_side(3)
+    hop_far(2)
     token_hop(1, 2)
-    token_hop(0, 3)
-    hop_far(2)
-    hop_far(3)
     weights_in()
+    tokens_in(0)
     feed(0)
     down(0)
-    token_hop(1, 3)
+    tokens_in(1)
     feed(1)
     down(1)
     collect(0)
@@ -689,6 +713,9 @@
                         return carry
 
                     lax.fori_loop(0, blocks, drain, 0)
+
+    for part in range(2):
+        result(part).wait()
 
 
 def rotary_tables(tok_rows, head_size):
@@ -720,8 +747,9 @@
         functools.partial(layer_kernel, n, tn),
         out_shape=jax.ShapeDtypeStruct((rows, wide), b16),
         in_specs=[vmem, vmem, hbm, vmem, vmem, vmem, vmem, hbm, vmem, vmem, vmem, hbm, hbm, hbm, vmem],
-        out_specs=vmem,
+        out_specs=hbm,
         scratch_shapes=[
+            pltpu.VMEM((rows, wide), b16),
             pltpu.VMEM((tok, hd), f32),
             pltpu.VMEM((tok, hd), f32),
             pltpu.VMEM((groups, hd, tok), b16),
@@ -744,7 +772,7 @@
             pltpu.VMEM((2, half * rows // 2, wide), f32),
             pltpu.VMEM((2, 2, half - 1, rows // 2, wide), b16),
             pltpu.VMEM((2, 2, half - 1, rows // 2, wide), b16),
-            pltpu.SemaphoreType.DMA((6,)),
+            pltpu.SemaphoreType.DMA((8,)),
             pltpu.SemaphoreType.DMA((4 * half,)),
             pltpu.SemaphoreType.DMA((4 * half,)),
             pltpu.SemaphoreType.DMA((tn - 1,)),

time: 166 us -> 152 us (0.916); the launches traced: 163 us -> 151 us
  Pallas kernels: 160 us -> 149 us
    pallas_call x1, Pallas kernels: 160 us -> 149 us  [fused(): pl.pallas_call(functools.partial(layer_kernel, n, tn), out_shape=jax.Shap...]
where the time goes in v3:
time: 152 us; the launch traced here: 151 us
  Pallas kernels  149 us (98%)
  local copies, waits for them, and re-layouts  1.88 us (1%)
    pallas_call x1, Pallas kernels, fused(): pl.pallas_call(functools.partial(layer_kernel, n, tn), out_shape=jax.Shap...  149 us

profile of v3, /device:TPU:0, one launch (start us, length us, event | category | flops | bytes accessed | tf_op | source)
XLA Modules:
  0.0 151.4 jit_solution(16756137888806863683)
XLA Ops:
  0.0 0.8 negate_select_fusion
  0.9 148.6 %shard_map.127 = bf16[128,2048]{1,0:T(8,128)(2,1)} custom-call(bf16[512,512]{1,0:T(8,128)(2,1)} %q_in.1, bf16[512,128]{1,0:T(8,128)(2,1)} %k_in.1, bf16[512,128]{1,0:T(8,128)(2,1)} %v_hbm.1, f32[72,128]{1,0:T(8,128)} %get-tuple-element.6.cos_in, f32[72,128]{1,0:T(8,128)} %get-tuple-element.5.sin_in, f32[1,128]{1,0:T(1,128)} %bitcast.8, f32[1,128]{1,0:T(1,128)} %bitcast.9, ...), custom_call_target="tpu_custom_call" | custom-call | tf_op jit(solution)/shard_map/pallas_call | solution.py:746
  149.5 1.9 %copy.15 = bf16[128,2048]{1,0:T(8,128)(2,1)} copy(bf16[128,2048]{1,0:T(8,128)(2,1)} %shard_map.127) | data formatting | bytes 1048576
  (3 shorter events, 0.0 us)

commit v4 on v3

--- a/solution.py
+++ b/solution.py
@@ -138,16 +138,14 @@
 def layer_kernel(
     n,
     tn,
-    q_in,
+    q_hbm,
     k_in,
     v_hbm,
-    cos_in,
-    sin_in,
     qg_ref,
     kg_ref,
     ow_hbm,
     og_ref,
-    res_ref,
+    res_hbm,
     mg_ref,
     gate_hbm,
     up_hbm,
@@ -155,6 +153,8 @@
     fg_ref,
     out_hbm,
     out_ref,
+    q_in,
+    res_ref,
     cos_ref,
     sin_ref,
     qs,
@@ -174,6 +174,7 @@
     mid,
     toks,
     inner,
+    partial,
     osc,
     psend,
     precv,
@@ -231,7 +232,9 @@
         "d": pltpu.make_async_copy(down_hbm, wt.at[2], loc_sem.at[3]),
         "o": pltpu.make_async_copy(ow_hbm, ow, loc_sem.at[4]),
     }
-    for name in "vgudo":
+    locs["q"] = pltpu.make_async_copy(q_hbm, q_in, loc_sem.at[8])
+    locs["r"] = pltpu.make_async_copy(res_hbm, res_ref, loc_sem.at[9])
+    for name in "vguqdor":
         locs[name].start()
 
     lane = lax.broadcasted_iota(jnp.int32, (tok, hd), 1)
@@ -244,21 +247,23 @@
         other = jnp.where(first, pltpu.roll(x, hd - quarter, 1), pltpu.roll(x, quarter, 1))
         return (x * cos_ref[...] + other * sin_ref[...]).astype(jnp.bfloat16)
 
+    grid_rows = tok // GRID_W
+    shape = (grid_rows + GRID_W, hd)
+    index = lax.broadcasted_iota(jnp.int32, shape, 0)
+    spot = lax.broadcasted_iota(jnp.int32, shape, 1)
+    freqs = jnp.exp(lax.rem(spot, quarter).astype(jnp.float32) * (-math.log(10000.0) / quarter))
+    place = jnp.where(index < grid_rows, sp * grid_rows + index, index - grid_rows)
+    angle = place.astype(jnp.float32) * freqs
+    sine = jnp.sin(angle)
+    turn = jnp.where(lax.rem(spot, 2 * quarter) < quarter, -sine, sine)
     low = lane[:GRID_W] < 2 * quarter
-    grid_rows = tok // GRID_W
-    for row in range(grid_rows):
-        part = slice(row * GRID_W, (row + 1) * GRID_W)
-        for small, large in ((cos_in, cos_ref), (sin_in, sin_ref)):
+    for small, large in ((jnp.cos(angle), cos_ref), (turn, sin_ref)):
+        for row in range(grid_rows):
+            part = slice(row * GRID_W, (row + 1) * GRID_W)
             large[part, :] = jnp.where(low, small[row : row + 1, :], small[grid_rows:, :])
     kbuf[sp] = turned(k_in[...], kg_ref[...])
 
     pl.semaphore_wait(barrier, n - 1 + tn - 1)
-
-    started = []
-
-    def start(copy):
-        copy.start()
-        started.append(copy)
 
     items = {
         "k": (0, half, lambda s: kbuf.at[s]),
@@ -271,7 +276,7 @@
         return pltpu.make_async_remote_copy(
             src_ref=view(origin),
             dst_ref=view(origin),
-            send_sem=send_sem.at[index],
+            send_sem=send_sem.at[number],
             recv_sem=recv_sem.at[index],
             device_id=(right if way == 0 else left, tp),
             device_id_type=MESH,
@@ -283,7 +288,7 @@
 
     def send(name):
         for way, count in counts(name):
-            start(ring_copy(name, way, 1, sp))
+            ring_copy(name, way, 1, sp).start()
 
     def arrive(name, step):
         for way, count in counts(name):
@@ -292,9 +297,15 @@
             origin = ring_at(pos - step) if way == 0 else ring_at(pos + step)
             ring_copy(name, way, step, origin).wait_recv()
             if step < count:
-                start(ring_copy(name, way, step + 1, origin))
-
-    bases = {"z": 0, "x": 1, "y": 2, "d": 3, "cz": 4, "cy": 5, "cx": 6, "cd": 7}
+                ring_copy(name, way, step + 1, origin).start()
+
+    last = 2
+
+    def w_index(kind, k, which):
+        if kind[0] == "c":
+            return 4 * nz * 3 + (1 if k == last else 0)
+        return ("zxyd".index(kind) * nz + k) * 3 + which
+
     whole = [(0, 3)]
     thirds = [(0, 1), (1, 1), (2, 1)]
 
@@ -311,7 +322,6 @@
         return wall.at[slot, part[0] : part[0] + part[1], r * hq : (r + 1) * hq, :]
 
     def weight_copy(kind, k, part):
-        index = (bases[kind] * nz + k) * 3 + part[0]
         if kind == "x":
             slot, r_from, r_to, dev = column(k, y), 0, 2, x_dev
         elif kind == "y":
@@ -327,70 +337,66 @@
         return pltpu.make_async_remote_copy(
             src_ref=piece(slot, r_from, part),
             dst_ref=piece(slot, r_to, part),
-            send_sem=w_send.at[index],
-            recv_sem=w_recv.at[index],
+            send_sem=w_send.at[2 if kind[0] == "c" else 1],
+            recv_sem=w_recv.at[w_index(kind, k, part[0])],
             device_id=dev,
             device_id_type=MESH,
         )
 
     def weight_wait(kind, k, part):
-        side = y if kind in ("z", "x", "cz", "cx") else other_y
-        r = {"z": 0, "y": 0, "x": 2, "d": 2, "cz": 1, "cy": 1, "cx": 3, "cd": 3}[kind]
+        side = y if kind in ("z", "x") else other_y
         for small in parts(kind, k):
             if small[0] < part[0] or small[0] >= part[0] + part[1]:
                 continue
-            index = (bases[kind] * nz + k) * 3 + small[0]
-            here = piece(column(k, side), r, small)
-            pltpu.make_async_remote_copy(
-                src_ref=here,
-                dst_ref=here,
-                send_sem=w_send.at[index],
-                recv_sem=w_recv.at[index],
-                device_id=c_dev,
-                device_id_type=MESH,
-            ).wait_recv()
+            here = piece(column(k, side), 0 if kind in ("z", "y") else 2, small)
+            arrival(here, w_recv.at[w_index(kind, k, small[0])]).wait_recv()
+
+    def arrival(ref, semaphore):
+        return pltpu.make_async_remote_copy(
+            src_ref=ref,
+            dst_ref=ref,
+            send_sem=semaphore,
+            recv_sem=semaphore,
+            device_id=c_dev,
+            device_id_type=MESH,
+        )
 
     spread_list = [(k, which) for k in (1, 3, 2) for which in range(3)]
 
     def spread(count):
         for k, which in spread_list[:count]:
             target = lax.rem(z - k + nz, nz)
-            index = (bases["z"] * nz + k) * 3 + which
-            start(
-                pltpu.make_async_remote_copy(
-                    src_ref=wt.at[
-                        which : which + 1, pl.ds(pl.multiple_of(target * hq, 16), hq), :
-                    ],
-                    dst_ref=wall.at[sp, which : which + 1, 0:hq, :],
-                    send_sem=w_send.at[index],
-                    recv_sem=w_recv.at[index],
-                    device_id=(2 * target + y, tp),
-                    device_id_type=MESH,
-                )
-            )
+            pltpu.make_async_remote_copy(
+                src_ref=wt.at[which : which + 1, pl.ds(pl.multiple_of(target * hq, 16), hq), :],
+                dst_ref=wall.at[sp, which : which + 1, 0:hq, :],
+                send_sem=w_send.at[0],
+                recv_sem=w_recv.at[w_index("z", k, which)],
+                device_id=(2 * target + y, tp),
+                device_id_type=MESH,
+            ).start()
         del spread_list[:count]
 
     def hop_own(k, some=(0, 1, 2)):
         for which in some:
             weight_wait("z", k, thirds[which])
             for kind in ("y", "x", "cz"):
-                start(weight_copy(kind, k, thirds[which]))
+                weight_copy(kind, k, thirds[which]).start()
 
     def hop_side(k, some=(0, 1, 2)):
         for which in some:
             for kind, route in (("y", "x"), ("x", "y")):
                 weight_wait(kind, k, thirds[which])
                 if diagonal(k, which) == route:
-                    start(weight_copy("d", k, thirds[which]))
-                start(weight_copy("c" + kind, k, thirds[which]))
+                    weight_copy("d", k, thirds[which]).start()
+                weight_copy("c" + kind, k, thirds[which]).start()
 
     def hop_far(k, some=(0, 1, 2)):
         for which in some:
             weight_wait("d", k, thirds[which])
             if k > 0:
-                start(weight_copy("cd", k, thirds[which]))
+                weight_copy("cd", k, thirds[which]).start()
         if k == 0:
-            start(weight_copy("cd", k, whole[0]))
+            weight_copy("cd", k, whole[0]).start()
 
     send("k")
     locs["v"].wait()
@@ -411,12 +417,13 @@
         wt.at[:, pl.ds(pl.multiple_of(z * hq, 16), hq), :], wall.at[sp, :, 0:hq, :], loc_sem.at[5]
     )
     own_piece.start()
-    spread(1)
+    spread(2)
     own_piece.wait()
-    start(weight_copy("x", 0, whole[0]))
-    start(weight_copy("cz", 0, whole[0]))
-    start(weight_copy("y", 0, thirds[0]))
-
+    weight_copy("x", 0, whole[0]).start()
+    weight_copy("cz", 0, whole[0]).start()
+    weight_copy("y", 0, thirds[0]).start()
+
+    locs["q"].wait()
     for h in range(groups):
         qs[h] = turned(q_in[:, h * hd : (h + 1) * hd], qg_ref[...]).T
     m_s[...] = jnp.full_like(m_s, -1e30)
@@ -449,17 +456,19 @@
         arrive("k", step)
         arrive("v", step)
         if step != half - 1:
-            spread(1 if step < half else 4)
+            spread(1 if step < half else 3)
         if step < 3:
-            start(weight_copy("y", 0, thirds[step]))
+            weight_copy("y", 0, thirds[step]).start()
+        if step == 2:
+            hop_own(1, (0, 1))
         if step <= 3:
             weight_wait("y", 0, thirds[step - 1])
-            start(weight_copy("d", 0, thirds[step - 1]))
+            weight_copy("d", 0, thirds[step - 1]).start()
         if step == half - 1:
-            start(weight_copy("cy", 0, whole[0]))
+            weight_copy("cy", 0, whole[0]).start()
             weight_wait("x", 0, whole[0])
-            start(weight_copy("cx", 0, whole[0]))
-            hop_own(1)
+            weight_copy("cx", 0, whole[0]).start()
+            hop_own(1, (2,))
         ends = [ring_at(pos - step), ring_at(pos + step)]
         attend(ends if step < half else ends[:1])
 
@@ -467,26 +476,24 @@
         done = (acc[h] / l_s[h]).astype(jnp.bfloat16)
         for t in range(tn):
             att[t, :, h * hd : (h + 1) * hd] = done[:, t * rows : (t + 1) * rows].T
-    to_heads = []
     for d in range(1, tn):
         peer = lax.rem(tp + d, tn)
         copy = pltpu.make_async_remote_copy(
             src_ref=att.at[peer],
             dst_ref=heads.at[tp],
-            send_sem=tp_send.at[d - 1],
-            recv_sem=tp_recv.at[d - 1],
+            send_sem=tp_send.at[0],
+            recv_sem=tp_recv.at[0],
             device_id=(sp, peer),
             device_id_type=MESH,
         )
         copy.start()
-        to_heads.append(copy)
     heads[tp] = att[tp]
     hop_far(0)
     hop_side(1)
     hop_own(3, (0, 1))
     locs["o"].wait()
-    for copy in to_heads:
-        copy.wait_recv()
+    locs["r"].wait()
+    arrival(heads.at[0 : tn - 1], tp_recv.at[0]).wait_recv()
 
     span = math.gcd(ow.shape[1], 512)
 
@@ -524,7 +531,7 @@
     def token_copy(part, way, e, lag):
         origin = z - (e - lag) if way == 0 else z + (e - lag)
         block = toks.at[part, line_rows(origin), :]
-        index = (part * 2 + way) * nz + e
+        index = (part * 2 + way) * (nz - 1) + e - 1
         return pltpu.make_async_remote_copy(
             src_ref=block,
             dst_ref=block,
@@ -561,106 +568,110 @@
                 for e in range(1, nz):
                     token_copy(part, way, e, 0).wait_recv()
 
-    def weights_in():
-        for k in range(nz):
-            for kind in ("cz", "cy", "cx", "cd"):
-                weight_wait(kind, k, (0, 3))
-
-    def feed(part):
+    def weights_in(late):
+        arrival(wall.at[0 : 1 if late else nz - 1], w_recv.at[w_index("c", last if late else 0, 0)]).wait_recv()
+
+    def feed(part, blocks, before=False, after=True):
         def feed_tile(r, carry):
             base = pl.multiple_of(r * hq, 16)
             branches = []
             for which in range(2):
                 total = jnp.zeros((hq, nz * side), jnp.float32)
-                for s in range(n):
+                for s in blocks:
                     total += lax.dot_general(
                         wall[s, which, pl.ds(base, hq), :],
-                        toks[part, :, s * depth : (s + 1) * depth],
+                        toks[part, :, pl.ds(pl.multiple_of(s * depth, 128), depth)],
                         (((1,), (1,)), ((), ())),
                         preferred_element_type=jnp.float32,
                     )
-                branches.append(total)
-            gate, up = branches
-            inner[pl.ds(base, hq), :] = (gate / (1.0 + jnp.exp(-gate)) * up).astype(jnp.bfloat16)
+                if before:
+                    total += partial[which, pl.ds(base, hq), :]
+                if after:
+                    branches.append(total)
+                else:
+                    partial[which, pl.ds(base, hq), :] = total
+            if after:
+                gate, up = branches
+                inner[pl.ds(base, hq), :] = (gate / (1.0 + jnp.exp(-gate)) * up).astype(jnp.bfloat16)
             return carry
 
         lax.fori_loop(0, tn, feed_tile, 0)
 
-    blocks = 1
-    cut = wide // blocks
-
-    def columns(j):
-        return pl.ds(pl.multiple_of(j * cut, 128), cut)
-
-    def sum_copy(part, way, d, j):
-        index = ((part * 2 + way) * nz + d) * blocks + j
+    early = [column(k, at) for k in range(nz) if k != last for at in range(2)]
+    late = [column(last, at) for at in range(2)]
+
+    cut = wide // 2
+    halves = [slice(0, cut), slice(cut, wide)]
+    full = [slice(0, wide)]
+
+    def sum_copy(part, way, d, cols):
+        index = (((part * 2 + way) * (nz - 1)) + d - 1) * 2 + cols.start // cut
         return pltpu.make_async_remote_copy(
-            src_ref=psend.at[part, way, d - 1, :, columns(j)],
-            dst_ref=precv.at[part, way, d - 1, :, columns(j)],
+            src_ref=psend.at[part, way, d - 1, :, cols],
+            dst_ref=precv.at[part, way, d - 1, :, cols],
             send_sem=p_send.at[index],
             recv_sem=p_recv.at[index],
             device_id=next_dev[way],
             device_id_type=MESH,
         )
 
-    def sum_wait(part, way, d, j):
-        sum_copy(part, way, d + 1, j).wait_recv()
-
-    def share(part, way, d, j):
+    def share(part, way, d, cols):
         owner = z + d if way == 0 else z - d
-        return osc[part, line_rows(owner), columns(j)]
+        return osc[part, line_rows(owner), cols]
 
     def down(part):
-        def down_block(j, carry):
-            for which in range(cut // depth):
-                s = (cut // depth) * j + which
-                osc[part, :, pl.ds(pl.multiple_of(s * depth, 128), depth)] = lax.dot_general(
-                    inner[...],
-                    wall[s, 2],
-                    (((0,), (0,)), ((), ())),
-                    preferred_element_type=jnp.float32,
-                )
-            for way in range(2):
-
-                @pl.when(behind[way] == 0)
-                def _():
-                    for d in range(nz - 1, 0, -1):
-                        psend[part, way, d - 1, :, columns(j)] = share(part, way, d, j).astype(
+        for s in range(n):
+            osc[part, :, s * depth : (s + 1) * depth] = lax.dot_general(
+                inner[...],
+                wall[s, 2],
+                (((0,), (0,)), ((), ())),
+                preferred_element_type=jnp.float32,
+            )
+        for way in range(2):
+
+            @pl.when(behind[way] == 0)
+            def _():
+                for d in range(nz - 1, 0, -1):
+                    for cols in halves if d == nz - 1 else full:
+                        psend[part, way, d - 1, :, cols] = share(part, way, d, cols).astype(
                             jnp.bfloat16
                         )
-                        sum_copy(part, way, d, j).start()
-
-            return carry
-
-        lax.fori_loop(0, blocks, down_block, 0)
+                        sum_copy(part, way, d, cols).start()
+
+    def pass_sums(part, way, d, pieces):
+        for cols in pieces:
+            sum_copy(part, way, d + 1, cols).wait_recv()
+            psend[part, way, d - 1, :, cols] = (
+                share(part, way, d, cols) + precv[part, way, d, :, cols].astype(jnp.float32)
+            ).astype(jnp.bfloat16)
+            sum_copy(part, way, d, cols).start()
 
     def collect(part):
         mine = slice(part * side, (part + 1) * side)
-
-        def collect_block(j, carry):
-            for d in range(nz - 2, 0, -1):
-                for way in range(2):
-
-                    @pl.when(jnp.logical_and(behind[way] > 0, ahead[way] >= d))
-                    def _():
-                        sum_wait(part, way, d, j)
-                        psend[part, way, d - 1, :, columns(j)] = (
-                            share(part, way, d, j)
-                            + precv[part, way, d, :, columns(j)].astype(jnp.float32)
-                        ).astype(jnp.bfloat16)
-                        sum_copy(part, way, d, j).start()
-
-            proj[mine, columns(j)] = share(part, 0, 0, j)
+        for d in range(nz - 2, 0, -1):
             for way in range(2):
 
-                @pl.when(behind[way] > 0)
+                @pl.when(jnp.logical_and(behind[way] > 0, ahead[way] == d))
                 def _():
-                    sum_wait(part, way, 0, j)
-                    proj[mine, columns(j)] += precv[part, way, 0, :, columns(j)].astype(jnp.float32)
-
-            return carry
-
-        lax.fori_loop(0, blocks, collect_block, 0)
+                    pass_sums(part, way, d, halves)
+
+        for d in range(nz - 2, 0, -1):
+            for way in range(2):
+
+                @pl.when(jnp.logical_and(behind[way] > 0, ahead[way] > d))
+                def _():
+                    pass_sums(part, way, d, full)
+
+        proj[mine] = share(part, 0, 0, full[0])
+        for way in range(2):
+            for pieces in (halves, full):
+
+                @pl.when(jnp.logical_and(behind[way] > 0, ahead[way] == 0 if pieces is halves else ahead[way] > 0))
+                def _():
+                    for cols in pieces:
+                        sum_copy(part, way, 1, cols).wait_recv()
+                        proj[mine, cols] += precv[part, way, 0, :, cols].astype(jnp.float32)
+
         total = proj[mine]
         out_ref[mine] = (
             mid[mine].astype(jnp.float32)
@@ -676,27 +687,35 @@
     hop_own(3, (2,))
     hop_far(1)
     token_hop(0, 1)
-    hop_side(3)
-    hop_own(2)
+    hop_side(3, (0,))
+    hop_own(2, (0,))
+    hop_side(3, (1, 2))
+    hop_own(2, (1, 2))
     token_hop(0, 2)
     hop_side(2, (0,))
     token_send(1)
     hop_side(2, (1, 2))
     hop_far(3)
+    weights_in(False)
+    tokens_in(0)
+    feed(0, early, after=False)
     token_hop(1, 1)
     hop_far(2)
     token_hop(1, 2)
-    weights_in()
-    tokens_in(0)
-    feed(0)
+    weights_in(True)
+    feed(0, late, before=True)
     down(0)
     tokens_in(1)
-    feed(1)
+    feed(1, range(n))
     down(1)
     collect(0)
     collect(1)
-    for copy in started + to_heads:
-        copy.wait_send()
+    arrival(kbuf.at[0 : n - 1], send_sem.at[0]).wait_send()
+    arrival(vbuf.at[0 : n - 1], send_sem.at[1]).wait_send()
+    arrival(att.at[0 : tn - 1], tp_send.at[0]).wait_send()
+    arrival(wall.at[0, :, 0 : (nz - 1) * hq, :], w_send.at[0]).wait_send()
+    arrival(wall.at[0 : nz - 1], w_send.at[1]).wait_send()
+    arrival(wall.at[0:nz], w_send.at[2]).wait_send()
 
     for part in range(2):
         for way in range(2):
@@ -706,29 +725,15 @@
                 def _():
                     token_copy(part, way, e, 1).wait_send()
 
-                @pl.when(ahead[way] >= e)
-                def _():
-                    def drain(j, carry):
-                        sum_copy(part, way, e, j).wait_send()
-                        return carry
-
-                    lax.fori_loop(0, blocks, drain, 0)
+                for pieces in (halves, full):
+
+                    @pl.when(ahead[way] == e if pieces is halves else ahead[way] > e)
+                    def _():
+                        for cols in pieces:
+                            sum_copy(part, way, e, cols).wait_send()
 
     for part in range(2):
         result(part).wait()
-
-
-def rotary_tables(tok_rows, head_size):
-    quarter = head_size // 4
-    grid_rows = tok_rows // GRID_W
-    lane = jnp.arange(head_size, dtype=jnp.int32)
-    freqs = 10000.0 ** (-(lane % quarter).astype(jnp.float32) / quarter)
-    index = jnp.arange(grid_rows + GRID_W, dtype=jnp.int32)
-    base = lax.axis_index("sp") * grid_rows
-    place = jnp.where(index < grid_rows, base + index, index - grid_rows)
-    angle = place.astype(jnp.float32)[:, None] * freqs
-    sine = jnp.sin(angle)
-    return jnp.cos(angle), jnp.where(lane % (2 * quarter) < quarter, -sine, sine)
 
 
 def fused(n, tn, *args):
@@ -738,7 +743,6 @@
     groups = queries.shape[1] // hd
     depth, hidden = gate_weight.shape
     rows, wide = residual_in.shape
-    cosine, sine = rotary_tables(tok, hd)
     vmem = pl.BlockSpec(memory_space=pltpu.VMEM)
     hbm = pl.BlockSpec(memory_space=pl.ANY)
     half = n // 2
@@ -746,9 +750,11 @@
     return pl.pallas_call(
         functools.partial(layer_kernel, n, tn),
         out_shape=jax.ShapeDtypeStruct((rows, wide), b16),
-        in_specs=[vmem, vmem, hbm, vmem, vmem, vmem, vmem, hbm, vmem, vmem, vmem, hbm, hbm, hbm, vmem],
+        in_specs=[hbm, vmem, hbm, vmem, vmem, hbm, vmem, hbm, vmem, hbm, hbm, hbm, vmem],
         out_specs=hbm,
         scratch_shapes=[
+            pltpu.VMEM((rows, wide), b16),
+            pltpu.VMEM((tok, groups * hd), b16),
             pltpu.VMEM((rows, wide), b16),
             pltpu.VMEM((tok, hd), f32),
             pltpu.VMEM((tok, hd), f32),
@@ -769,20 +775,21 @@
             pltpu.VMEM((rows, wide), b16),
             pltpu.VMEM((2, half * rows // 2, wide), b16),
             pltpu.VMEM((hidden // half * tn, half * rows // 2), b16),
+            pltpu.VMEM((2, hidden // half * tn, half * rows // 2), f32),
             pltpu.VMEM((2, half * rows // 2, wide), f32),
             pltpu.VMEM((2, 2, half - 1, rows // 2, wide), b16),
             pltpu.VMEM((2, 2, half - 1, rows // 2, wide), b16),
-            pltpu.SemaphoreType.DMA((8,)),
+            pltpu.SemaphoreType.DMA((10,)),
+            pltpu.SemaphoreType.DMA((2,)),
             pltpu.SemaphoreType.DMA((4 * half,)),
-            pltpu.SemaphoreType.DMA((4 * half,)),
-            pltpu.SemaphoreType.DMA((tn - 1,)),
-            pltpu.SemaphoreType.DMA((tn - 1,)),
-            pltpu.SemaphoreType.DMA((8 * half * 3,)),
-            pltpu.SemaphoreType.DMA((8 * half * 3,)),
-            pltpu.SemaphoreType.DMA((2 * half * 2,)),
-            pltpu.SemaphoreType.DMA((2 * half * 2,)),
-            pltpu.SemaphoreType.DMA((8 * half,)),
-            pltpu.SemaphoreType.DMA((8 * half,)),
+            pltpu.SemaphoreType.DMA((1,)),
+            pltpu.SemaphoreType.DMA((1,)),
+            pltpu.SemaphoreType.DMA((3,)),
+            pltpu.SemaphoreType.DMA((4 * half * 3 + 2,)),
+            pltpu.SemaphoreType.DMA((4 * (half - 1),)),
+            pltpu.SemaphoreType.DMA((4 * (half - 1),)),
+            pltpu.SemaphoreType.DMA((8 * (half - 1),)),
+            pltpu.SemaphoreType.DMA((8 * (half - 1),)),
         ],
         compiler_params=pltpu.CompilerParams(
             collective_id=0, has_side_effects=True, vmem_limit_bytes=67043328
@@ -791,8 +798,6 @@
         queries,
         keys,
         values,
-        cosine,
-        sine,
         q_gain[None],
         k_gain[None],
         out_weight,

time: 152 us -> 144 us (0.947)
  Pallas kernels: 149 us -> 140 us
    pallas_call x1, Pallas kernels: 149 us -> 140 us  [fused(): pl.pallas_call(functools.partial(layer_kernel, n, tn), out_shape=jax.Shap...]
where the time goes in v4:
time: 144 us; the launch traced here: 142 us
  Pallas kernels  140 us (97%)
  local copies, waits for them, and re-layouts  1.88 us (1%)
    pallas_call x1, Pallas kernels, fused(): pl.pallas_call(functools.partial(layer_kernel, n, tn), out_shape=jax.Shap...  140 us

profile of v4, /device:TPU:0, one launch (start us, length us, event | category | flops | bytes accessed | tf_op | source)
XLA Modules:
  0.0 142.1 jit_solution(10876863501633769516)
XLA Ops:
  0.0 140.2 %shard_map.127 = bf16[128,2048]{1,0:T(8,128)(2,1)} custom-call(bf16[512,512]{1,0:T(8,128)(2,1)} %q_hbm.1, bf16[512,128]{1,0:T(8,128)(2,1)} %k_in.1, bf16[512,128]{1,0:T(8,128)(2,1)} %v_hbm.1, f32[1,128]{1,0:T(1,128)} %bitcast.8, f32[1,128]{1,0:T(1,128)} %bitcast.9, bf16[2048,2048]{1,0:T(8,128)(2,1)} %ow_hbm.1, f32[1,2048]{1,0:T(1,128)} %bitcast.5, ...), custom_call_target="tpu_custom_call" | custom-call | tf_op jit(solution)/shard_map/pallas_call | solution.py:750
  140.2 1.9 %copy.15 = bf16[128,2048]{1,0:T(8,128)(2,1)} copy(bf16[128,2048]{1,0:T(8,128)(2,1)} %shard_map.127) | data formatting | bytes 1048576
